TPU v7x, 256 devices: a whole 4x4x8 slice. The times are simulated.
256 devices in a mesh: ep: 16 (over y, x), tp: 16 (over z, core).
Axes of the slice: x: 4, y: 4, z: 8, core: 2. Of those that a mesh axis runs over, the one named last changes fastest.
Arguments:
- query_rows: bfloat16 [2048, 2048], P('ep', 'tp'), may hold values from -32 to 32
- key_rows: bfloat16 [2048, 2048], P('ep', 'tp'), may hold values from -8 to 8
- value_rows: bfloat16 [2048, 2048], P('ep', 'tp'), may hold values from -8 to 8
- query_norm_gain: float32 [64], replicated, may hold values from 0.1 to 1.9
- key_gain: float32 [64], replicated, may hold values from 0.1 to 1.9
- break_offset: float32 [32], P('tp'), may hold values from -12 to 3
- mixer_out_weight: bfloat16 [2048, 2048], P('tp'), may hold values from -0.75 to 0.75
- routed_tokens: bfloat16 [32768, 2048], P(('ep', 'tp')), may hold values from -6 to 6
- expert_gain: float32 [2048], replicated, may hold values from 0.1 to 1.9
- routes: int32 [32768, 2], P(('ep', 'tp')), may hold values from 0 to 15, as said below
- route_scores: float32 [32768, 2], P(('ep', 'tp')), may hold values from -6 to 6
- gate_weight: bfloat16 [16, 2048, 3584], P('ep', None, 'tp'), may hold values from -0.125 to 0.125
- up_weight: bfloat16 [16, 2048, 3584], P('ep', None, 'tp'), may hold values from -0.125 to 0.125
- down_weight: bfloat16 [16, 3584, 2048], P('ep', 'tp'), may hold values from -0.09375 to 0.09375
Outputs:
- attention_output: bfloat16 [2048, 2048], P(('ep', 'tp'))
- expert_output: bfloat16 [32768, 2048], P(('ep', 'tp'))
Inputs may be any that keep to these rules, and one draw needn't show every extreme that they name: `routes`: each row names 2 different experts. Among the rows of one device no expert is named more than 16 times, and one expert is named exactly 16 times by the rows of every device.
All inputs are finite; a program needn't handle non-finite values.
Results may differ from a plain program's by a relative error of at most 0.018.
Values may be sent and summed in bfloat16 or wider, within the bound.
A program may use at most 128 MiB of HBM per device.

v0:
```python
import jax
import jax.numpy as jnp
from jax import lax
from jax.sharding import PartitionSpec as P

HEAD_DIM = 64
TOP_K = 2


EPS = 1e-06


def shifted(array, axis, by):
    peers = lax.axis_size(axis)
    pairs = [(i, i + by) for i in range(peers) if 0 <= i + by < peers]
    return lax.ppermute(array, axis, pairs)


def norm_heads(flat, gain):
    count = flat.shape[0]
    split = flat.astype(jnp.float32).reshape(count, -1, HEAD_DIM)
    scaled = split * lax.rsqrt(jnp.mean(split * split, axis=2, keepdims=True) + EPS)
    return (scaled * gain).astype(jnp.bfloat16)


def absorb(carry_state, query_norm, key_flat, value_flat, offsets, allowed):
    running_sum, carried = carry_state
    key_count = key_flat.shape[0]
    key_norm = key_flat.reshape(key_count, -1, HEAD_DIM)
    value_heads = value_flat.reshape(key_count, -1, HEAD_DIM)
    scores = jnp.einsum("qhd,khd->hqk", query_norm, key_norm, preferred_element_type=jnp.float32)
    scores = scores * HEAD_DIM ** (-0.5) + offsets[:, None, None]
    log_rise = jax.nn.log_sigmoid(scores)
    log_fail = jnp.where(allowed[None], log_rise - scores, 0.0)
    log_after = carried[:, :, None] + lax.cumsum(log_fail, axis=2, reverse=True) - log_fail
    weights = jnp.where(allowed[None], jnp.exp(log_rise + log_after), 0.0).astype(jnp.bfloat16)
    running_sum = running_sum + jnp.einsum(
        "hqk,khd->qhd", weights, value_heads, preferred_element_type=jnp.float32
    )
    return (running_sum, carried + jnp.sum(log_fail, axis=2))


def body(
    query_rows,
    key_rows,
    value_rows,
    query_norm_gain,
    key_gain,
    break_offset,
    mixer_out_weight,
    routed_tokens,
    expert_gain,
    routes,
    route_scores,
    gate_weight,
    up_weight,
    down_weight,
):
    gate_local = gate_weight[0]
    up_local = up_weight[0]
    down_local = down_weight[0]
    row_count = query_rows.shape[0]
    query_norm = norm_heads(query_rows, query_norm_gain)
    head_count = query_norm.shape[1]
    key_flat = norm_heads(key_rows, key_gain).reshape(row_count, -1)
    my_index = lax.axis_index("ep")
    devices_ep = lax.axis_size("ep")
    token_position = jnp.arange(row_count)
    earlier = token_position[None, :] < token_position[:, None]
    carry_state = (
        jnp.zeros((row_count, head_count, HEAD_DIM), jnp.float32),
        jnp.zeros((head_count, row_count), jnp.float32),
    )
    carry_state = absorb(carry_state, query_norm, key_flat, value_rows, break_offset, earlier)
    held_keys = key_flat[None]
    held_values = value_rows[None]
    for bit_level in range(devices_ep.bit_length() - 1):
        far_keys, far_values = shifted((held_keys, held_values), "ep", 2**bit_level)
        held_keys = jnp.concatenate([held_keys, far_keys], axis=0)
        held_values = jnp.concatenate([held_values, far_values], axis=0)

    def visit(turn_index, state_now):
        allowed = jnp.broadcast_to(my_index >= turn_index, (row_count, row_count))
        return absorb(
            state_now,
            query_norm,
            held_keys[turn_index],
            held_values[turn_index],
            break_offset,
            allowed,
        )

    carry_state = lax.fori_loop(1, devices_ep, visit, carry_state)
    heads_mixed = carry_state[0].astype(jnp.bfloat16).reshape(row_count, -1)
    token_count = routed_tokens.shape[0]
    model_width = routed_tokens.shape[1]
    as_float = routed_tokens.astype(jnp.float32)
    normed = (
        as_float
        * lax.rsqrt(jnp.mean(as_float * as_float, axis=1, keepdims=True) + EPS)
        * expert_gain
    ).astype(jnp.bfloat16)
    expert_count = lax.axis_size("ep")
    capacity = max(2, token_count * TOP_K // expert_count)
    flat_routes = routes.reshape(-1)
    member = (flat_routes[:, None] == jnp.arange(expert_count, dtype=jnp.int32)[None, :]).astype(
        jnp.int32
    )
    ahead = jnp.sum((jnp.cumsum(member, axis=0) - member) * member, axis=1)
    slot_index = flat_routes * capacity + ahead
    select = (
        slot_index[:, None] == jnp.arange(expert_count * capacity, dtype=jnp.int32)[None, :]
    ).astype(jnp.bfloat16)
    copies = jnp.repeat(normed, TOP_K, axis=0)
    outgoing = jnp.einsum("cs,cd->sd", select, copies, preferred_element_type=jnp.float32).astype(
        jnp.bfloat16
    )
    arrived = lax.all_to_all(outgoing, "ep", split_axis=0, concat_axis=0, tiled=True)
    slab = arrived.shape[0]
    devices_tp = lax.axis_size("tp")
    mixer_share = row_count // devices_tp
    piece = lax.all_gather(arrived, "tp", axis=0, tiled=True)
    gate_piece = jnp.dot(piece, gate_local, preferred_element_type=jnp.float32)
    up_piece = jnp.dot(piece, up_local, preferred_element_type=jnp.float32)
    hidden = (jax.nn.silu(gate_piece) * up_piece).astype(jnp.bfloat16)
    span = mixer_share + slab
    block_number = lax.axis_size("tp") * span // span
    mixer_term = jnp.dot(heads_mixed, mixer_out_weight, preferred_element_type=jnp.float32)
    expert_term = jnp.dot(hidden, down_local, preferred_element_type=jnp.float32)
    joined = jnp.concatenate(
        [
            mixer_term.reshape(block_number, mixer_share, -1),
            expert_term.reshape(block_number, slab, -1),
        ],
        axis=1,
    )
    summed = lax.psum_scatter(
        joined.reshape(block_number * span, -1).astype(jnp.bfloat16),
        "tp",
        scatter_dimension=0,
        tiled=True,
    ).astype(jnp.float32)
    mixer_sum = summed[:mixer_share]
    expert_sum = summed[mixer_share:]
    returned = lax.all_to_all(
        expert_sum.astype(jnp.bfloat16), "ep", split_axis=0, concat_axis=0, tiled=True
    )
    results = jnp.einsum("cs,sd->cd", select, returned, preferred_element_type=jnp.float32)
    results = results.reshape(token_count, TOP_K, model_width)
    differences = route_scores[:, None, :] - route_scores[:, :, None]
    route_weight = 1.0 / jnp.sum(jnp.exp(differences), axis=2)
    expert_output = jnp.sum(route_weight[..., None] * results, axis=1).astype(jnp.bfloat16)
    return (mixer_sum.astype(jnp.bfloat16), expert_output)


def solution(mesh):
    in_specs = (
        P("ep", "tp"),
        P("ep", "tp"),
        P("ep", "tp"),
        P(),
        P(),
        P("tp"),
        P("tp", None),
        P(("ep", "tp"), None),
        P(),
        P(("ep", "tp"), None),
        P(("ep", "tp"), None),
        P("ep", None, "tp"),
        P("ep", None, "tp"),
        P("ep", "tp", None),
    )
    out_specs = (P(("ep", "tp"), None), P(("ep", "tp"), None))
    return jax.shard_map(body, mesh=mesh, in_specs=in_specs, out_specs=out_specs, check_vma=False)
```

profile of v0, /device:TPU:6, one launch (start us, length us, event | category | flops | bytes accessed | tf_op | source)
XLA Modules:
  0.0 304.2 jit_solution(6313708067219499604)
XLA Ops:
  13.5 21.9 %all_to_all.24 = bf16[16,16,2048]{2,1,0:T(8,128)(2,1)} all-to-all(bf16[16,16,2048]{2,1,0:T(8,128)(2,1)S(1)} %bitcast.96), channel_id=1, replica_groups=mesh['ep'=16,'tp'=16] {'ep'}, dimensions={0} | all-to-all | bytes 2097152 | tf_op jit(solution)/shard_map/all_to_all | solution.py:118
  35.8 3.4 %collective-permute-start.4 = (bf16[1,128,128]{1,2,0:T(8,128)(2,1)S(1)}, bf16[1,128,128]{1,2,0:T(8,128)(2,1)S(1)}, u32[]{:S(2)}, u32[]{:S(2)}) collective-permute-start(bf16[1,128,128]{1,2,0:T(8,128)(2,1)S(1)} %bitcast.106), channel_id=1, source_target_pairs={{0,16},{16,32},{32,48},{48,64},{64,80},{80,96},{96,112},{112,128},... | collective-permute-start | bytes 98312 | tf_op jit(solution)/shard_map/ppermute | solution.py:16
  39.3 2.5 collective-permute-start
  42.5 2.2 reduce_window_sum.38
  45.0 3.8 %collective-permute-start.5 = (bf16[2,128,128]{1,2,0:T(8,128)(2,1)S(1)}, bf16[2,128,128]{1,2,0:T(8,128)(2,1)S(1)}, u32[]{:S(2)}, u32[]{:S(2)}) collective-permute-start(bf16[2,128,128]{1,2,0:T(8,128)(2,1)S(1)} %pad_maximum_fusion.6), channel_id=1, source_target_pairs={{0,32},{16,48},{32,64},{48,80},{64,96},{80,112},{96,128},{112,144}... | collective-permute-start | bytes 196616 | tf_op jit(solution)/shard_map/ppermute | solution.py:16
  48.8 4.5 %collective-permute-start.1 = (bf16[2,128,128]{1,2,0:T(8,128)(2,1)S(1)}, bf16[2,128,128]{1,2,0:T(8,128)(2,1)S(1)}, u32[]{:S(2)}, u32[]{:S(2)}) collective-permute-start(bf16[2,128,128]{1,2,0:T(8,128)(2,1)S(1)} %pad_maximum_fusion.5), channel_id=1, source_target_pairs={{0,32},{16,48},{32,64},{48,80},{64,96},{80,112},{96,128},{112,144}... | collective-permute-start | bytes 196616 | tf_op jit(solution)/shard_map/ppermute | solution.py:16
  53.4 3.4 %collective-permute-start.6 = (bf16[4,128,128]{1,2,0:T(8,128)(2,1)S(1)}, bf16[4,128,128]{1,2,0:T(8,128)(2,1)S(1)}, u32[]{:S(2)}, u32[]{:S(2)}) collective-permute-start(bf16[4,128,128]{1,2,0:T(8,128)(2,1)S(1)} %pad_maximum_fusion.4), channel_id=1, source_target_pairs={{0,64},{16,80},{32,96},{48,112},{64,128},{80,144},{96,160},{112,17... | collective-permute-start | bytes 393224 | tf_op jit(solution)/shard_map/ppermute | solution.py:16
  56.8 3.3 %collective-permute-start.2 = (bf16[4,128,128]{1,2,0:T(8,128)(2,1)S(1)}, bf16[4,128,128]{1,2,0:T(8,128)(2,1)S(1)}, u32[]{:S(2)}, u32[]{:S(2)}) collective-permute-start(bf16[4,128,128]{1,2,0:T(8,128)(2,1)S(1)} %pad_maximum_fusion.3), channel_id=1, source_target_pairs={{0,64},{16,80},{32,96},{48,112},{64,128},{80,144},{96,160},{112,17... | collective-permute-start | bytes 393224 | tf_op jit(solution)/shard_map/ppermute | solution.py:16
  60.2 5.4 %collective-permute-start.7 = (bf16[8,128,128]{1,2,0:T(8,128)(2,1)S(1)}, bf16[8,128,128]{1,2,0:T(8,128)(2,1)S(1)}, u32[]{:S(2)}, u32[]{:S(2)}) collective-permute-start(bf16[8,128,128]{1,2,0:T(8,128)(2,1)S(1)} %pad_maximum_fusion.2), channel_id=1, source_target_pairs={{0,128},{16,144},{32,160},{48,176},{64,192},{80,208},{96,224},{112... | collective-permute-start | bytes 786440 | tf_op jit(solution)/shard_map/ppermute | solution.py:16
  65.7 3.0 collective-permute-start.3
  70.8 2.8 collective-permute-done.3
  73.6 43.0 %while.17 = (s32[]{:T(128)}, f32[128,2,64]{0,2,1:T(8,128)S(1)}, f32[2,128]{1,0:T(2,128)S(1)}, bf16[16,128,128]{1,2,0:T(8,128)(2,1)S(1)}, s32[]{:T(128)}, /*index...) while((s32[]{:T(128)}, f32[128,2,64]{0,2,1:T(8,128)S(1)}, ...), condition=%wide.region_7.8_spmd, body=%wide.region_4.7_spmd.sunk | while | flops 13484038 | bytes 1152186 | solution.py:93
  82.7 2.2 reduce_window_sum.44
  85.6 2.2 reduce_window_sum.44
  99.9 2.2 reduce_window_sum.44
  117.2 14.9 %all-gather.2.cloned.1.call-done = bf16[4096,2048]{1,0:T(8,128)(2,1)} async-done(((bf16[256,2048]{1,0:T(8,128)(2,1)}), bf16[4096,2048]{1,0:T(8,128)(2,1)}) %all-gather.2.cloned.1.call-update) | async-done | bytes 16777232 | tf_op jit(solution)/shard_map/all_gather | solution.py:122
  132.1 10.5 %fusion.17 = f32[4096,224]{0,1:T(8,128)S(1)} fusion(bf16[4096,2048]{1,0:T(8,128)(2,1)} %all-gather.2.cloned.1.call-done, bf16[1,2048,224]{1,2,0:T(8,128)(2,1)} %param.27), kind=kOutput, calls=%fused_computation.34 | convolution fusion | flops 3758096384 | bytes 21364736 | tf_op jit(solution)/shard_map/dot_general | solution.py:123
  143.1 5.4 %fusion.7 = bf16[4096,224]{0,1:T(8,128)(2,1)S(1)} fusion(bf16[4096,2048]{1,0:T(8,128)(2,1)S(1)} %copy-done.8, f32[4096,224]{0,1:T(8,128)S(1)} %fusion.17, bf16[1,2048,224]{1,2,0:T(8,128)(2,1)S(1)} %copy-done.9), kind=kOutput, calls=%fused_computation.17 | convolution fusion | flops 3763601408 | bytes 23199744 | tf_op jit(solution)/shard_map/dot_general | solution.py:124
  148.6 8.2 %convolution_convert_fusion = bf16[16,256,2048]{2,1,0:T(8,128)(2,1)} fusion(bf16[28,16,8,256]{3,2,1,0:T(8,128)(2,1)S(1)} %bitcast.97, bf16[1,224,2048]{2,1,0:T(8,128)(2,1)S(1)} %copy-done), kind=kOutput, calls=%fused_computation.15 | convolution fusion | flops 3766484992 | bytes 19529728 | tf_op jit(solution)/shard_map/dot_general | solution.py:129
  156.7 14.3 %pad_maximum_fusion = bf16[16,264,2048]{2,1,0:T(8,128)(2,1)} fusion(bf16[16,256,2048]{2,1,0:T(8,128)(2,1)} %convolution_convert_fusion, bf16[16,8,2048]{2,1,0:T(8,128)(2,1)S(1)} %convolution_convert_fusion.2), kind=kLoop, calls=%fused_computation.14 | loop fusion | flops 34603008 | bytes 34603008 | tf_op jit(solution)/shard_map/concatenate | solution.py:130
  171.1 101.8 %reduce-scatter.2.cloned.1.call-done = bf16[264,2048]{1,0:T(8,128)(2,1)} async-done(((bf16[4224,2048]{1,0:T(8,128)(2,1)}), bf16[264,2048]{1,0:T(8,128)(2,1)}) %reduce-scatter.2.cloned.1.call-update) | async-done | bytes 1081360 | tf_op jit(solution)/shard_map/reduce_scatter | solution.py:137
  272.9 2.3 slice.20
  275.3 7.3 %all-to-all-start.1 = ((bf16[16,16,2048]{2,1,0:T(8,128)(2,1)}), bf16[16,16,2048]{2,1,0:T(8,128)(2,1)S(1)}, u32[]{:S(2)}, u32[]{:S(2)}) async-start(bf16[16,16,2048]{2,1,0:T(8,128)(2,1)} %bitcast.21), calls=%async_computation.2 | async-start | bytes 2097152 | tf_op jit(solution)/shard_map/all_to_all | solution.py:145
  284.2 11.8 %all-to-all-done.1 = bf16[16,16,2048]{2,1,0:T(8,128)(2,1)S(1)} async-done(((bf16[16,16,2048]{2,1,0:T(8,128)(2,1)}), bf16[16,16,2048]{2,1,0:T(8,128)(2,1)S(1)}, u32[]{:S(2)}, u32[]{:S(2)}) %all-to-all-start.1) | async-done | bytes 1048608 | tf_op jit(solution)/shard_map/all_to_all | solution.py:145
  (164 shorter events, 49.4 us)
Async XLA Ops:
  7.2 141.4 %copy-start = (bf16[1,224,2048]{2,1,0:T(8,128)(2,1)S(1)}, bf16[1,224,2048]{2,1,0:T(8,128)(2,1)}, u32[]{:S(2)}) copy-start(bf16[1,224,2048]{2,1,0:T(8,128)(2,1)} %param.29) | copy-start | bytes 2752516
  7.2 125.0 %all-gather.2.cloned.1.call-start = ((), (), s32[]{:S(2)}) async-start(), calls=%async_computation.3 | async-start | bytes 17825792 | tf_op jit(solution)/shard_map/all_gather | solution.py:122
  12.4 23.0 %copy-start.3 = (bf16[128,128]{1,0:T(8,128)(2,1)S(1)}, bf16[128,128]{1,0:T(8,128)(2,1)}, u32[]{:S(2)}) copy-start(bf16[128,128]{1,0:T(8,128)(2,1)} %param.17) | copy-start | bytes 98308
  12.4 23.1 %copy-start.10 = (f32[64]{0:T(128)S(1)}, f32[64]{0:T(128)}, u32[]{:S(2)}) copy-start(f32[64]{0:T(128)} %param.20) | copy-start | bytes 772
  12.4 26.8 %copy-start.4 = (bf16[128,128]{1,0:T(8,128)(2,1)S(1)}, bf16[128,128]{1,0:T(8,128)(2,1)}, u32[]{:S(2)}) copy-start(bf16[128,128]{1,0:T(8,128)(2,1)} %param.18) | copy-start | bytes 98308
  12.5 29.4 %copy-start.2 = (bf16[128,128]{1,0:T(8,128)(2,1)S(1)}, bf16[128,128]{1,0:T(8,128)(2,1)}, u32[]{:S(2)}) copy-start(bf16[128,128]{1,0:T(8,128)(2,1)} %param.16) | copy-start | bytes 98308
  12.5 29.5 %copy-start.7 = (f32[64]{0:T(128)S(1)}, f32[64]{0:T(128)}, u32[]{:S(2)}) copy-start(f32[64]{0:T(128)} %param.19) | copy-start | bytes 772
  12.5 29.6 %copy-start.11 = (f32[2]{0:T(128)S(1)}, f32[2]{0:T(128)}, u32[]{:S(2)}) copy-start(f32[2]{0:T(128)} %param.21) | copy-start | bytes 28
  35.4 237.6 %reduce-scatter.2.cloned.1.call-start = ((), (), s32[]{:S(2)}) async-start(), calls=%async_computation.4 | async-start | bytes 18382848 | tf_op jit(solution)/shard_map/reduce_scatter | solution.py:137
  35.8 9.2 %collective-permute-start.4 = (bf16[1,128,128]{1,2,0:T(8,128)(2,1)S(1)}, bf16[1,128,128]{1,2,0:T(8,128)(2,1)S(1)}, u32[]{:S(2)}, u32[]{:S(2)}) collective-permute-start(bf16[1,128,128]{1,2,0:T(8,128)(2,1)S(1)} %bitcast.106), channel_id=1, source_target_pairs={{0,16},{16,32},{32,48},{48,64},{64,80},{80,96},{96,112},{112,128},... | collective-permute-start | bytes 98312 | tf_op jit(solution)/shard_map/ppermute | solution.py:16
  39.3 9.5 %collective-permute-start = (bf16[1,128,128]{1,2,0:T(8,128)(2,1)S(1)}, bf16[1,128,128]{1,2,0:T(8,128)(2,1)S(1)}, u32[]{:S(2)}, u32[]{:S(2)}) collective-permute-start(bf16[1,128,128]{1,2,0:T(8,128)(2,1)S(1)} %bitcast.99), channel_id=1, source_target_pairs={{0,16},{16,32},{32,48},{48,64},{64,80},{80,96},{96,112},{112,128},... | collective-permute-start | bytes 98312 | tf_op jit(solution)/shard_map/ppermute | solution.py:16
  45.0 8.3 %collective-permute-start.5 = (bf16[2,128,128]{1,2,0:T(8,128)(2,1)S(1)}, bf16[2,128,128]{1,2,0:T(8,128)(2,1)S(1)}, u32[]{:S(2)}, u32[]{:S(2)}) collective-permute-start(bf16[2,128,128]{1,2,0:T(8,128)(2,1)S(1)} %pad_maximum_fusion.6), channel_id=1, source_target_pairs={{0,32},{16,48},{32,64},{48,80},{64,96},{80,112},{96,128},{112,144}... | collective-permute-start | bytes 196616 | tf_op jit(solution)/shard_map/ppermute | solution.py:16
  48.8 7.9 %collective-permute-start.1 = (bf16[2,128,128]{1,2,0:T(8,128)(2,1)S(1)}, bf16[2,128,128]{1,2,0:T(8,128)(2,1)S(1)}, u32[]{:S(2)}, u32[]{:S(2)}) collective-permute-start(bf16[2,128,128]{1,2,0:T(8,128)(2,1)S(1)} %pad_maximum_fusion.5), channel_id=1, source_target_pairs={{0,32},{16,48},{32,64},{48,80},{64,96},{80,112},{96,128},{112,144}... | collective-permute-start | bytes 196616 | tf_op jit(solution)/shard_map/ppermute | solution.py:16
  53.4 6.8 %collective-permute-start.6 = (bf16[4,128,128]{1,2,0:T(8,128)(2,1)S(1)}, bf16[4,128,128]{1,2,0:T(8,128)(2,1)S(1)}, u32[]{:S(2)}, u32[]{:S(2)}) collective-permute-start(bf16[4,128,128]{1,2,0:T(8,128)(2,1)S(1)} %pad_maximum_fusion.4), channel_id=1, source_target_pairs={{0,64},{16,80},{32,96},{48,112},{64,128},{80,144},{96,160},{112,17... | collective-permute-start | bytes 393224 | tf_op jit(solution)/shard_map/ppermute | solution.py:16
  56.8 8.9 %collective-permute-start.2 = (bf16[4,128,128]{1,2,0:T(8,128)(2,1)S(1)}, bf16[4,128,128]{1,2,0:T(8,128)(2,1)S(1)}, u32[]{:S(2)}, u32[]{:S(2)}) collective-permute-start(bf16[4,128,128]{1,2,0:T(8,128)(2,1)S(1)} %pad_maximum_fusion.3), channel_id=1, source_target_pairs={{0,64},{16,80},{32,96},{48,112},{64,128},{80,144},{96,160},{112,17... | collective-permute-start | bytes 393224 | tf_op jit(solution)/shard_map/ppermute | solution.py:16
  60.2 10.5 %collective-permute-start.7 = (bf16[8,128,128]{1,2,0:T(8,128)(2,1)S(1)}, bf16[8,128,128]{1,2,0:T(8,128)(2,1)S(1)}, u32[]{:S(2)}, u32[]{:S(2)}) collective-permute-start(bf16[8,128,128]{1,2,0:T(8,128)(2,1)S(1)} %pad_maximum_fusion.2), channel_id=1, source_target_pairs={{0,128},{16,144},{32,160},{48,176},{64,192},{80,208},{96,224},{112... | collective-permute-start | bytes 786440 | tf_op jit(solution)/shard_map/ppermute | solution.py:16
  65.7 7.8 %collective-permute-start.3 = (bf16[8,128,128]{1,2,0:T(8,128)(2,1)S(1)}, bf16[8,128,128]{1,2,0:T(8,128)(2,1)S(1)}, u32[]{:S(2)}, u32[]{:S(2)}) collective-permute-start(bf16[8,128,128]{1,2,0:T(8,128)(2,1)S(1)} %pad_maximum_fusion.1), channel_id=1, source_target_pairs={{0,128},{16,144},{32,160},{48,176},{64,192},{80,208},{96,224},{112... | collective-permute-start | bytes 786440 | tf_op jit(solution)/shard_map/ppermute | solution.py:16
  73.6 43.3 %copy-start.1 = (bf16[128,2048]{1,0:T(8,128)(2,1)S(1)}, bf16[128,2048]{1,0:T(8,128)(2,1)}, u32[]{:S(2)}) copy-start(bf16[128,2048]{1,0:T(8,128)(2,1)} %param.22) | copy-start | bytes 1572868
  132.1 10.8 %copy-start.8 = (bf16[4096,2048]{1,0:T(8,128)(2,1)S(1)}, bf16[4096,2048]{1,0:T(8,128)(2,1)}, u32[]{:S(2)}) copy-start(bf16[4096,2048]{1,0:T(8,128)(2,1)} %all-gather.2.cloned.1.call-done) | copy-start | bytes 50331652
  132.1 11.0 %copy-start.9 = (bf16[1,2048,224]{1,2,0:T(8,128)(2,1)S(1)}, bf16[1,2048,224]{1,2,0:T(8,128)(2,1)}, u32[]{:S(2)}) copy-start(bf16[1,2048,224]{1,2,0:T(8,128)(2,1)} %param.28) | copy-start | bytes 2752516
  171.1 111.7 %copy-start.6 = (f32[128,2]{0,1:T(2,128)S(1)}, f32[128,2]{0,1:T(2,128)}, u32[]{:S(2)}) copy-start(f32[128,2]{0,1:T(2,128)} %param.26) | copy-start | bytes 3076
  171.1 111.7 %copy-start.5 = (s32[128,2]{0,1:T(2,128)S(1)}, s32[128,2]{0,1:T(2,128)}, u32[]{:S(2)}) copy-start(s32[128,2]{0,1:T(2,128)} %param.25) | copy-start | bytes 3076
  275.3 20.7 %all-to-all-start.1 = ((bf16[16,16,2048]{2,1,0:T(8,128)(2,1)}), bf16[16,16,2048]{2,1,0:T(8,128)(2,1)S(1)}, u32[]{:S(2)}, u32[]{:S(2)}) async-start(bf16[16,16,2048]{2,1,0:T(8,128)(2,1)} %bitcast.21), calls=%async_computation.2 | async-start | bytes 2097152 | tf_op jit(solution)/shard_map/all_to_all | solution.py:145
Sparse Core Ops, SparseCore 0:
  35.5 96.5 all-gather.1
  171.2 101.7 reduce-scatter.1
where the time goes:
time: 309 us; the launch traced here: 304 us
  waiting for transfers between devices  133 us (43%)
  other arithmetic  53.7 us (17%)
  starting transfers between devices  36.6 us (12%)
  matrix products  35.3 us (11%)
  blocking collectives  21.9 us (7%)
  between operations  14.6 us (5%)
  local copies, waits for them, and re-layouts  7.83 us (3%)
    reduce_scatter x1, waiting for transfers between devices, body(): lax.psum_scatter(joined.reshape(block_number * span, -1).astype(jnp.bfloa...  102 us
    another operation x16, other arithmetic, absorb(): lax.cumsum(log_fail, axis=2, reverse=True)  35.5 us
    ppermute x8, starting transfers between devices, shifted(): return lax.ppermute(array, axis, pairs)  29.3 us
    all_to_all x1, blocking collectives, body(): lax.all_to_all(outgoing, 'ep', split_axis=0, concat_axis=0, tiled=True)  21.9 us
    all_gather x1, waiting for transfers between devices, body(): piece = lax.all_gather(arrived, 'tp', axis=0, tiled=True)  14.9 us
    concatenate x1, other arithmetic, body(): jnp.concatenate([mixer_term.reshape(block_number, mixer_share, -1), exper...  14.3 us
    all_to_all x1, waiting for transfers between devices, body(): lax.all_to_all(expert_sum.astype(jnp.bfloat16), 'ep', split_axis=0, conca...  11.8 us
    dot_general x1, matrix products, body(): gate_piece = jnp.dot(piece, gate_local, preferred_element_type=jnp.float32)  10.5 us
  transfers between devices with their start and end apart: 11, of which 5 were waited for; matrix products, arithmetic and copies ran while one was open for 16% of the time, Pallas kernels for 0%

commit v1 on v0

v1 whole, which is shorter than its diff:
```python
import functools

import jax
import jax.numpy as jnp
from jax import lax
from jax.experimental import pallas as pl
from jax.experimental.pallas import tpu as pltpu
from jax.sharding import PartitionSpec as P

HEAD_DIM = 64
EPS = 1e-06
MESH = pl.DeviceIdType.MESH
EP = 16
NZ = 8
CAP = 16
HALF = EP // 2
F32 = jnp.float32
BF16 = jnp.bfloat16


def iota(shape, dim):
    return lax.broadcasted_iota(jnp.int32, shape, dim)


def kernel(
    query_ref,
    key_ref,
    value_ref,
    query_gain_ref,
    key_gain_ref,
    offset_ref,
    mixer_hbm,
    tokens_ref,
    expert_gain_ref,
    routes_ref,
    scores_ref,
    gate_hbm,
    up_hbm,
    down_hbm,
    attn_out,
    expert_out,
    gate_w,
    up_w,
    down_w,
    mixer_w,
    kv,
    tok,
    slots,
    outgoing,
    arrived,
    terms,
    ring_out,
    ring_in,
    returned,
    mix_mine,
    mix_theirs,
    mix_out,
    mix_in,
    load_sem,
    pair_send,
    pair_recv,
    kv_send,
    kv_recv,
    up_send,
    up_recv,
    dn_send,
    dn_recv,
    slot_send,
    slot_recv,
    disp_send,
    disp_recv,
    ring_send,
    ring_recv,
    ret_send,
    ret_recv,
    mix_send,
    mix_recv,
):
    ep = lax.axis_index("ep")
    tp = lax.axis_index("tp")
    z, core = tp // 2, tp % 2
    above = (ep, lax.rem(z + 1, NZ) * 2 + core)
    below = (ep, lax.rem(z + NZ - 1, NZ) * 2 + core)
    sibling = (ep, z * 2 + 1 - core)
    rows = query_ref.shape[0]
    tokens, width = tokens_ref.shape

    def remote(src, dst, send, recv, device):
        return pltpu.make_async_remote_copy(
            src_ref=src,
            dst_ref=dst,
            send_sem=send,
            recv_sem=recv,
            device_id=device,
            device_id_type=MESH,
        )

    barrier = pltpu.get_barrier_semaphore()

    def greet_ep(j, _):
        pl.semaphore_signal(
            barrier, inc=1, device_id=(lax.rem(ep + j, EP), tp), device_id_type=MESH
        )
        return 0

    def greet_z(j, _):
        pl.semaphore_signal(
            barrier,
            inc=1,
            device_id=(ep, lax.rem(z + j, NZ) * 2 + core),
            device_id_type=MESH,
        )
        return 0

    lax.fori_loop(1, EP, greet_ep, 0)
    lax.fori_loop(1, NZ, greet_z, 0)
    pl.semaphore_signal(barrier, inc=1, device_id=sibling, device_id_type=MESH)

    weights = ((gate_hbm, gate_w), (up_hbm, up_w), (down_hbm, down_w), (mixer_hbm, mixer_w))
    loads = [
        pltpu.make_async_copy(src, dst.at[0], load_sem.at[i])
        for i, (src, dst) in enumerate(weights)
    ]
    for copy in loads:
        copy.start()

    lane = iota((rows, 128), 1)
    first_head = lane < HEAD_DIM

    def norm_heads(flat, gain):
        split = flat.astype(F32)
        squares = split * split
        mean_a = jnp.sum(jnp.where(first_head, squares, 0.0), axis=1, keepdims=True) / HEAD_DIM
        mean_b = jnp.sum(jnp.where(first_head, 0.0, squares), axis=1, keepdims=True) / HEAD_DIM
        scale = jnp.where(first_head, lax.rsqrt(mean_a + EPS), lax.rsqrt(mean_b + EPS))
        return (split * scale * gain).astype(BF16)

    key_norm = norm_heads(key_ref[...], key_gain_ref[...])
    kv[ep, 0] = key_norm
    kv[ep, 1] = value_ref[...]

    as_float = tokens_ref[...].astype(F32)
    mean = jnp.mean(as_float * as_float, axis=1, keepdims=True)
    tok[0] = (as_float * lax.rsqrt(mean + EPS) * expert_gain_ref[...]).astype(BF16)

    expert_lane = iota((tokens, 128), 1)
    route_a, route_b = routes_ref[:, 0:1], routes_ref[:, 1:2]
    member_a = jnp.where(route_a == expert_lane, 1.0, 0.0).astype(F32)
    member_b = jnp.where(route_b == expert_lane, 1.0, 0.0).astype(F32)
    lower = jnp.where(iota((tokens, tokens), 1) < iota((tokens, tokens), 0), 1.0, 0.0).astype(BF16)
    ahead_a = jnp.dot(lower, member_a.astype(BF16), preferred_element_type=F32)
    ahead_b = jnp.dot(lower, member_b.astype(BF16), preferred_element_type=F32)
    ahead_b = ahead_b + jnp.sum(member_a, axis=0, keepdims=True)
    expert_base = (expert_lane * CAP).astype(F32)
    slot_a = jnp.sum(member_a * (ahead_a + expert_base), axis=1, keepdims=True)
    slot_b = jnp.sum(member_b * (ahead_b + expert_base), axis=1, keepdims=True)
    slots[0, 0] = jnp.transpose(jnp.broadcast_to(slot_a, (tokens, 128)))[0:8]
    slots[0, 1] = jnp.transpose(jnp.broadcast_to(slot_b, (tokens, 128)))[0:8]

    pl.semaphore_wait(barrier, EP - 1 + NZ - 1 + 1)

    def ag_up(hop):
        return remote(tok.at[hop - 1], tok.at[hop], up_send.at[hop], up_recv.at[hop], above)

    def ag_down(hop):
        return remote(
            tok.at[lax.rem(NZ + 1 - hop, NZ)],
            tok.at[NZ - hop],
            dn_send.at[hop],
            dn_recv.at[hop],
            below,
        )

    half_tok = tokens // 2

    def last_up():
        part = pl.ds(0, half_tok)
        return remote(tok.at[3, part], tok.at[4, part], up_send.at[4], up_recv.at[4], above)

    def last_down():
        part = pl.ds(half_tok, half_tok)
        return remote(tok.at[5, part], tok.at[4, part], dn_send.at[4], dn_recv.at[4], below)

    def slot_copy(j):
        peer = (ep, lax.rem(z + j, NZ) * 2 + core)
        return remote(slots.at[0], slots.at[j], slot_send.at[j], slot_recv.at[j], peer)

    ag_up(1).start()
    ag_down(1).start()

    def send_slots(j, _):
        slot_copy(j).start()
        return 0

    lax.fori_loop(1, NZ, send_slots, 0)

    def kv_copy(source, target):
        return remote(
            kv.at[source], kv.at[source], kv_send.at[target], kv_recv.at[source], (target, tp)
        )

    def send_kv(j, _):
        kv_copy(ep, j).start()
        return 0

    lax.fori_loop(ep + 1, EP, send_kv, 0)

    pair_copies = [
        remote(src, dst.at[1], pair_send.at[i], pair_recv.at[i], sibling)
        for i, (src, dst) in enumerate(weights)
    ]
    for copy in pair_copies:
        copy.start()

    slot_rows = iota((EP * CAP, tokens), 0).astype(F32)

    def dispatch(step, distance):
        row_a = slots[distance, 0][0:1]
        row_b = slots[distance, 1][0:1]
        pick = jnp.where((slot_rows == row_a) | (slot_rows == row_b), 1.0, 0.0).astype(BF16)
        picked = jnp.dot(pick, tok[distance], preferred_element_type=F32).astype(BF16)
        outgoing[step] = picked.reshape(EP, CAP, width)

        def send(j, _):
            peer = lax.rem(ep + j, EP)
            remote(
                outgoing.at[step, peer],
                arrived.at[step, ep],
                disp_send.at[step],
                disp_recv.at[step],
                (peer, tp),
            ).start()
            return 0

        lax.fori_loop(1, EP, send, 0)
        arrived[step, ep] = outgoing[step, ep]

    def all_but_one(buffer, send, recv):
        block = buffer.at[pl.ds(0, EP - 1)]
        return remote(block, block, send, recv, sibling)

    dispatch(0, 0)

    def wait_slots(j, _):
        slot_copy(j).wait_recv()
        return 0

    lax.fori_loop(1, NZ, wait_slots, 0)

    def advance(step):
        @pl.when(step <= 3)
        def _():
            ag_up(step).wait_recv()

            @pl.when(step <= 2)
            def _():
                ag_up(step + 1).start()

            @pl.when(step == 3)
            def _():
                last_up().start()

            ag_down(step).wait_recv()

            @pl.when(step <= 2)
            def _():
                ag_down(step + 1).start()

            @pl.when(step == 3)
            def _():
                last_down().start()

        @pl.when(step == 4)
        def _():
            last_up().wait_recv()
            last_down().wait_recv()

        dispatch(step, jnp.where(ep < HALF, step, NZ - step))

    def attention():
        query_norm = norm_heads(query_ref[...], query_gain_ref[...])
        zero = jnp.zeros_like(query_norm)
        queries = jnp.concatenate(
            [jnp.where(first_head, query_norm, zero), jnp.where(first_head, zero, query_norm)],
            axis=0,
        )
        row = iota((2 * rows, rows), 0)
        column = iota((2 * rows, rows), 1)
        offsets = jnp.where(row < rows, offset_ref[0], offset_ref[1])
        position = jnp.where(row < rows, row, row - rows)
        after = jnp.where(iota((rows, rows), 0) > iota((rows, rows), 1), 1.0, 0.0).astype(BF16)

        def absorb(j, state):
            mixed, carried = state

            @pl.when(j < ep)
            def _():
                kv_copy(j, ep).wait_recv()

            keys, values = kv[j, 0], kv[j, 1]
            scores = lax.dot_general(
                queries, keys, (((1,), (1,)), ((), ())), preferred_element_type=F32
            )
            scores = scores * HEAD_DIM ** (-0.5) + offsets
            allowed = (column < position) | (j < ep)
            log_fail = -(jnp.maximum(scores, 0.0) + jnp.log1p(jnp.exp(-jnp.abs(scores))))
            log_rise = scores + log_fail
            log_fail = jnp.where(allowed, log_fail, 0.0)
            high = log_fail.astype(BF16)
            rest = log_fail - high.astype(F32)
            middle = rest.astype(BF16)
            low = (rest - middle.astype(F32)).astype(BF16)
            between = (
                jnp.dot(high, after, preferred_element_type=F32)
                + jnp.dot(middle, after, preferred_element_type=F32)
                + jnp.dot(low, after, preferred_element_type=F32)
            )
            weights = jnp.where(allowed, jnp.exp(log_rise + between + carried), 0.0).astype(BF16)
            mixed = mixed + jnp.dot(weights, values, preferred_element_type=F32)
            carried = carried + jnp.sum(log_fail, axis=1, keepdims=True)
            return mixed, carried

        state = (jnp.zeros((2 * rows, 128), F32), jnp.zeros((2 * rows, 1), F32))
        mixed, _ = lax.fori_loop(0, ep + 1, lambda t, s: absorb(ep - t, s), state)
        heads = jnp.where(first_head, mixed[:rows], mixed[rows:]).astype(BF16)
        to_row = iota((rows, rows), 0)
        from_row = iota((rows, rows), 1)
        owner_core = to_row // 64
        within = to_row % 64
        source = (within // 8) * 16 + owner_core * 8 + within % 8
        order = jnp.where(from_row == source, 1.0, 0.0).astype(BF16)
        ordered = jnp.dot(order, heads, preferred_element_type=F32).astype(BF16)
        mix_mine[0] = ordered[:64]
        mix_mine[1] = ordered[64:]

    def mix_pair():
        return remote(
            mix_mine.at[1 - core], mix_theirs, pair_send.at[4], pair_recv.at[4], sibling
        )

    def mix_terms():
        loads[3].wait()
        pair_copies[3].wait_recv()
        mix_pair().wait_recv()
        term = jnp.dot(mix_mine[core], mixer_w[0], preferred_element_type=F32)
        term = term + jnp.dot(mix_theirs[...], mixer_w[1], preferred_element_type=F32)
        for i in range(NZ):
            mix_out[i] = term[8 * i : 8 * i + 8].astype(BF16)

        def send(j, _):
            to = lax.rem(z + j, NZ)
            remote(mix_out.at[to], mix_in.at[j], mix_send, mix_recv, (ep, to * 2 + core)).start()
            return 0

        lax.fori_loop(1, NZ, send, 0)

    def experts(step):
        rows_in = arrived[lax.rem(step, NZ)].reshape(EP * CAP, width)
        total = None
        for i in range(2):
            gate = jnp.dot(rows_in, gate_w[i], preferred_element_type=F32)
            up = jnp.dot(rows_in, up_w[i], preferred_element_type=F32)
            hidden = (gate / (1.0 + jnp.exp(-gate)) * up).astype(BF16)
            term = jnp.dot(hidden, down_w[i], preferred_element_type=F32)
            total = term if total is None else total + term
        terms[...] = total

    def ring(step, part, device):
        return remote(
            ring_out.at[step, pl.ds(part * HALF, HALF)],
            ring_in.at[step + 1, pl.ds(part * HALF, HALF)],
            ring_send.at[part, step],
            ring_recv.at[part, step + 1],
            device,
        )

    half_rows = HALF * CAP

    def combine(step):
        for part, device in ((0, above), (1, below)):
            blocks = pl.ds(part * HALF, HALF)
            mine = terms[part * half_rows : (part + 1) * half_rows, :]

            @pl.when(step == 1)
            def _():
                ring_out[step, blocks] = mine.astype(BF16).reshape(HALF, CAP, width)

            @pl.when(step >= 2)
            def _():
                ring(step - 1, part, device).wait_recv()
                sofar = ring_in[step, blocks].reshape(half_rows, width).astype(F32)
                ring_out[step, blocks] = (mine + sofar).astype(BF16).reshape(HALF, CAP, width)

            @pl.when(step < NZ)
            def _():
                ring(step, part, device).start()

            @pl.when(step == NZ)
            def _():
                def send(j, _):
                    peer = part * HALF + j

                    @pl.when(peer != ep)
                    def _():
                        remote(
                            ring_out.at[NZ, peer],
                            returned.at[ep],
                            ret_send,
                            ret_recv,
                            (peer, tp),
                        ).start()

                    return 0

                lax.fori_loop(0, HALF, send, 0)

    advance(1)
    attention()
    mix_pair().start()
    for i in range(3):
        loads[i].wait()
        pair_copies[i].wait_recv()

    def one_step(step, _):
        @pl.when(step + 1 < NZ)
        def _():
            advance(step + 1)

        every = all_but_one(
            arrived.at[lax.rem(step, NZ)], disp_send.at[0], disp_recv.at[lax.rem(step, NZ)]
        )
        every.wait_recv()
        experts(step)
        combine(step)

        @pl.when(step == 1)
        def _():
            mix_terms()

        return 0

    lax.fori_loop(1, NZ + 1, one_step, 0)
    returned[ep] = ring_out[NZ, ep]

    peers = mix_in.at[pl.ds(1, NZ - 1)]
    remote(peers, peers, mix_send, mix_recv, sibling).wait()
    total = mix_out[z].astype(F32)
    for j in range(1, NZ):
        total = total + mix_in[j].astype(F32)
    attn_out[...] = total.astype(BF16)

    slot_lane = iota((tokens, EP * CAP), 1).astype(F32)
    select_a = jnp.where(slot_lane == slot_a, 1.0, 0.0).astype(BF16)
    select_b = jnp.where(slot_lane == slot_b, 1.0, 0.0).astype(BF16)
    score_a, score_b = scores_ref[:, 0:1], scores_ref[:, 1:2]
    weight_a = 1.0 / (1.0 + jnp.exp(score_b - score_a))
    weight_b = 1.0 / (jnp.exp(score_a - score_b) + 1.0)
    all_but_one(returned, ret_send, ret_recv).wait()
    results = returned[...].reshape(EP * CAP, width)
    result_a = jnp.dot(select_a, results, preferred_element_type=F32)
    result_b = jnp.dot(select_b, results, preferred_element_type=F32)
    expert_out[...] = (weight_a * result_a + weight_b * result_b).astype(BF16)

    for hop in range(1, 4):
        ag_up(hop).wait_send()
        ag_down(hop).wait_send()
    last_up().wait_send()
    last_down().wait_send()
    mix_pair().wait_send()
    for copy in pair_copies:
        copy.wait_send()

    def drain_slots(j, _):
        slot_copy(j).wait_send()
        return 0

    lax.fori_loop(1, NZ, drain_slots, 0)

    def drain_kv(j, _):
        kv_copy(ep, j).wait_send()
        return 0

    lax.fori_loop(ep + 1, EP, drain_kv, 0)

    def drain_dispatch(step, _):
        all_but_one(outgoing.at[step], disp_send.at[step], disp_recv.at[step]).wait_send()
        return 0

    lax.fori_loop(0, NZ, drain_dispatch, 0)

    def drain_ring(step, _):
        ring(step, 0, above).wait_send()
        ring(step, 1, below).wait_send()
        return 0

    lax.fori_loop(1, NZ, drain_ring, 0)


def body(
    query_rows,
    key_rows,
    value_rows,
    query_norm_gain,
    key_gain,
    break_offset,
    mixer_out_weight,
    routed_tokens,
    expert_gain,
    routes,
    route_scores,
    gate_weight,
    up_weight,
    down_weight,
):
    rows = query_rows.shape[0]
    tokens, width = routed_tokens.shape
    units = gate_weight.shape[2]
    vmem = pl.BlockSpec(memory_space=pltpu.VMEM)
    smem = pl.BlockSpec(memory_space=pltpu.SMEM)
    hbm = pl.BlockSpec(memory_space=pl.ANY)
    dma = pltpu.SemaphoreType.DMA
    return pl.pallas_call(
        kernel,
        out_shape=(
            jax.ShapeDtypeStruct((rows // (2 * NZ), width), BF16),
            jax.ShapeDtypeStruct((tokens, width), BF16),
        ),
        in_specs=[vmem] * 5 + [smem, hbm] + [vmem] * 4 + [hbm] * 3,
        out_specs=(vmem, vmem),
        scratch_shapes=[
            pltpu.VMEM((2, width, units), BF16),
            pltpu.VMEM((2, width, units), BF16),
            pltpu.VMEM((2, units, width), BF16),
            pltpu.VMEM((2, 128, width), BF16),
            pltpu.VMEM((EP, 2, rows, 128), BF16),
            pltpu.VMEM((NZ, tokens, width), BF16),
            pltpu.VMEM((NZ, 2, 8, 128), F32),
            pltpu.VMEM((NZ, EP, CAP, width), BF16),
            pltpu.VMEM((NZ, EP, CAP, width), BF16),
            pltpu.VMEM((EP * CAP, width), F32),
            pltpu.VMEM((NZ + 1, EP, CAP, width), BF16),
            pltpu.VMEM((NZ + 1, EP, CAP, width), BF16),
            pltpu.VMEM((EP, CAP, width), BF16),
            pltpu.VMEM((2, 64, 128), BF16),
            pltpu.VMEM((64, 128), BF16),
            pltpu.VMEM((NZ, 8, width), BF16),
            pltpu.VMEM((NZ, 8, width), BF16),
            dma((4,)),
            dma((5,)),
            dma((5,)),
            dma((EP,)),
            dma((EP,)),
            dma((5,)),
            dma((5,)),
            dma((5,)),
            dma((5,)),
            dma((NZ,)),
            dma((NZ,)),
            dma((NZ,)),
            dma((NZ,)),
            dma((2, NZ + 1)),
            dma((2, NZ + 1)),
            dma,
            dma,
            dma,
            dma,
        ],
        compiler_params=pltpu.CompilerParams(
            collective_id=0, has_side_effects=True, vmem_limit_bytes=67043328
        ),
    )(
        query_rows,
        key_rows,
        value_rows,
        jnp.tile(query_norm_gain, 2)[None, :],
        jnp.tile(key_gain, 2)[None, :],
        break_offset,
        mixer_out_weight,
        routed_tokens,
        expert_gain[None, :],
        routes,
        route_scores,
        gate_weight[0],
        up_weight[0],
        down_weight[0],
    )


def solution(mesh):
    in_specs = (
        P("ep", "tp"),
        P("ep", "tp"),
        P("ep", "tp"),
        P(),
        P(),
        P("tp"),
        P("tp", None),
        P(("ep", "tp"), None),
        P(),
        P(("ep", "tp"), None),
        P(("ep", "tp"), None),
        P("ep", None, "tp"),
        P("ep", None, "tp"),
        P("ep", "tp", None),
    )
    out_specs = (P(("ep", "tp"), None), P(("ep", "tp"), None))
    return jax.shard_map(body, mesh=mesh, in_specs=in_specs, out_specs=out_specs, check_vma=False)
```

time: 309 us -> 179 us (0.58)
  Pallas kernels: 0 us -> 166 us
  waiting for transfers between devices: 133 us -> 0 us
  other arithmetic: 53.7 us -> 0 us
  starting transfers between devices: 36.6 us -> 0 us
  matrix products: 35.3 us -> 0 us
  blocking collectives: 21.9 us -> 0 us
  between operations: 14.6 us -> 0.65 us
    pallas_call x0 -> x1, Pallas kernels: none -> 166 us  [body(): pl.pallas_call(kernel, out_shape=(jax.ShapeDtypeStruct((rows // (2 * NZ),...]
    reduce_scatter x1 -> x0, waiting for transfers between devices: 102 us -> none  [body(): lax.psum_scatter(joined.reshape(block_number * span, -1).astype(jnp.bfloa...]
    another operation x18 -> x0, other arithmetic: 36.2 us -> none  [the longest x16 35.5 us: absorb(): lax.cumsum(log_fail, axis=2, reverse=True)]
    dot_general x38 -> x0, matrix products: 35.3 us -> none  [the longest x1 10.5 us: body(): gate_piece = jnp.dot(piece, gate_local, preferred_element_type=jnp.float32)]
    ppermute x8 -> x0, starting transfers between devices: 29.3 us -> none  [shifted(): return lax.ppermute(array, axis, pairs)]
    all_to_all x1 -> x0, blocking collectives: 21.9 us -> none  [body(): lax.all_to_all(outgoing, 'ep', split_axis=0, concat_axis=0, tiled=True)]
    all_gather x1 -> x0, waiting for transfers between devices: 14.9 us -> none  [body(): piece = lax.all_gather(arrived, 'tp', axis=0, tiled=True)]
    concatenate x7 -> x0, other arithmetic: 14.4 us -> none  [the longest x1 14.3 us: body(): jnp.concatenate([mixer_term.reshape(block_number, mixer_share, -1), exper...]
  transfers between devices with their start and end apart: 11 -> 0, of which waited for: 5 -> 0; matrix products, arithmetic and copies ran while one was open for 16% -> 0% of each run, Pallas kernels for 0% -> 0%
where the time goes in v1:
time: 179 us; the launch traced here: 177 us
  Pallas kernels  166 us (93%)
  local copies, waits for them, and re-layouts  10.3 us (6%)
    pallas_call x1, Pallas kernels, body(): pl.pallas_call(kernel, out_shape=(jax.ShapeDtypeStruct((rows // (2 * NZ),...  166 us
    unnamed x16, local copies, waits for them, and re-layouts  9.12 us

profile of v1, /device:TPU:6, one launch (start us, length us, event | category | flops | bytes accessed | tf_op | source)
XLA Modules:
  0.0 176.5 jit_solution(3397354052030424430)
XLA Ops:
  0.6 0.0 copy-start.3
  0.6 0.6 copy-done.3
  1.3 0.0 copy-start.4
  1.3 0.6 broadcast_in_dim_tile.6.query_gain_ref
  1.9 0.1 copy-done.4
  1.9 0.0 copy-start.1
  1.9 0.6 broadcast_in_dim_tile.7.key_gain_ref
  2.6 0.1 copy-done.1
  2.6 0.0 copy-start.2
  2.6 0.7 copy.18.routes_ref
  3.4 0.0 copy-done.2
  3.4 0.7 copy.19.scores_ref
  4.1 0.0 copy-start
  4.1 2.3 %copy.16 = bf16[1,2048,224]{2,1,0:T(8,128)(2,1)} copy(bf16[1,2048,224]{1,2,0:T(8,128)(2,1)} %param.25) | data formatting | bytes 1835008 | tf_op args[11]
  6.4 0.0 copy-done
  6.4 1.3 copy.17
  7.7 165.5 %shard_map.149 = (bf16[8,2048]{1,0:T(8,128)(2,1)}, bf16[128,2048]{1,0:T(8,128)(2,1)}) custom-call(bf16[128,128]{1,0:T(8,128)(2,1)} %query_ref.1, bf16[128,128]{1,0:T(8,128)(2,1)} %key_ref.1, bf16[128,128]{1,0:T(8,128)(2,1)} %value_ref.1, f32[1,128]{1,0:T(1,128)} %broadcast_in_dim_tile.6.query_gain_ref, f32[1,128]{1,0:T(1,128)} %broadcast_in_dim_tile.7.key_gain_ref, ...), custom_call_target="tpu_custom_call" | custom-call | tf_op jit(solution)/shard_map/pallas_call | solution.py:522
  173.3 1.4 copy.22
  174.7 1.9 %copy.23 = bf16[128,2048]{1,0:T(8,128)(2,1)} copy(bf16[128,2048]{1,0:T(8,128)(2,1)} %get-tuple-element.5) | data formatting | bytes 1048576
  (2 shorter events, 0.0 us)
Async XLA Ops:
  0.6 0.7 copy-start.3
  1.3 0.7 copy-start.4
  1.9 0.7 copy-start.1
  2.6 0.7 copy-start.2
  4.1 2.3 %copy-start = (bf16[1,2048,224]{1,2,0:T(8,128)(2,1)S(1)}, bf16[1,2048,224]{1,2,0:T(8,128)(2,1)}, u32[]{:S(2)}) copy-start(bf16[1,2048,224]{1,2,0:T(8,128)(2,1)} %param.26) | copy-start | bytes 2752516

commit v2 on v1

--- a/solution.py
+++ b/solution.py
@@ -84,6 +84,11 @@
     sibling = (ep, z * 2 + 1 - core)
     rows = query_ref.shape[0]
     tokens, width = tokens_ref.shape
+    position_here = lax.rem(ep // 4 + ep % 4, 4) * 4 + ep // 4
+    goes_up = position_here < HALF
+
+    def at_position(place):
+        return place % 4 * 4 + lax.rem(place // 4 + 4 - place % 4, 4)
 
     def remote(src, dst, send, recv, device):
         return pltpu.make_async_remote_copy(
@@ -133,7 +138,7 @@
         mean_a = jnp.sum(jnp.where(first_head, squares, 0.0), axis=1, keepdims=True) / HEAD_DIM
         mean_b = jnp.sum(jnp.where(first_head, 0.0, squares), axis=1, keepdims=True) / HEAD_DIM
         scale = jnp.where(first_head, lax.rsqrt(mean_a + EPS), lax.rsqrt(mean_b + EPS))
-        return (split * scale * gain).astype(BF16)
+        return (split * scale * jnp.concatenate([gain, gain], axis=1)).astype(BF16)
 
     key_norm = norm_heads(key_ref[...], key_gain_ref[...])
     kv[ep, 0] = key_norm
@@ -143,56 +148,57 @@
     mean = jnp.mean(as_float * as_float, axis=1, keepdims=True)
     tok[0] = (as_float * lax.rsqrt(mean + EPS) * expert_gain_ref[...]).astype(BF16)
 
-    expert_lane = iota((tokens, 128), 1)
-    route_a, route_b = routes_ref[:, 0:1], routes_ref[:, 1:2]
-    member_a = jnp.where(route_a == expert_lane, 1.0, 0.0).astype(F32)
-    member_b = jnp.where(route_b == expert_lane, 1.0, 0.0).astype(F32)
-    lower = jnp.where(iota((tokens, tokens), 1) < iota((tokens, tokens), 0), 1.0, 0.0).astype(BF16)
-    ahead_a = jnp.dot(lower, member_a.astype(BF16), preferred_element_type=F32)
-    ahead_b = jnp.dot(lower, member_b.astype(BF16), preferred_element_type=F32)
-    ahead_b = ahead_b + jnp.sum(member_a, axis=0, keepdims=True)
-    expert_base = (expert_lane * CAP).astype(F32)
-    slot_a = jnp.sum(member_a * (ahead_a + expert_base), axis=1, keepdims=True)
-    slot_b = jnp.sum(member_b * (ahead_b + expert_base), axis=1, keepdims=True)
-    slots[0, 0] = jnp.transpose(jnp.broadcast_to(slot_a, (tokens, 128)))[0:8]
-    slots[0, 1] = jnp.transpose(jnp.broadcast_to(slot_b, (tokens, 128)))[0:8]
-
-    pl.semaphore_wait(barrier, EP - 1 + NZ - 1 + 1)
-
-    def ag_up(hop):
-        return remote(tok.at[hop - 1], tok.at[hop], up_send.at[hop], up_recv.at[hop], above)
-
-    def ag_down(hop):
+    expert_row = iota((EP, tokens), 0)
+    member_a = jnp.where(routes_ref[0:1, :] == expert_row, 1.0, 0.0).astype(F32)
+    member_b = jnp.where(routes_ref[1:2, :] == expert_row, 1.0, 0.0).astype(F32)
+    earlier = jnp.where(iota((tokens, tokens), 0) < iota((tokens, tokens), 1), 1.0, 0.0)
+    earlier = earlier.astype(BF16)
+    ahead_a = jnp.dot(member_a.astype(BF16), earlier, preferred_element_type=F32)
+    ahead_b = jnp.dot(member_b.astype(BF16), earlier, preferred_element_type=F32)
+    ahead_b = ahead_b + jnp.sum(member_a, axis=1, keepdims=True)
+    expert_base = (expert_row * CAP).astype(F32)
+    slot_a = jnp.sum(member_a * (ahead_a + expert_base), axis=0, keepdims=True)
+    slot_b = jnp.sum(member_b * (ahead_b + expert_base), axis=0, keepdims=True)
+    slots[0, 0] = jnp.broadcast_to(slot_a, (8, tokens))
+    slots[0, 1] = jnp.broadcast_to(slot_b, (8, tokens))
+
+    with jax.named_scope("wait_entry"):
+        pl.semaphore_wait(barrier, EP - 1 + NZ - 1 + 1)
+
+    part_tok = tokens // 2
+
+    def ag_up(hop, chunk):
+        part = pl.ds(chunk * part_tok, part_tok)
         return remote(
-            tok.at[lax.rem(NZ + 1 - hop, NZ)],
-            tok.at[NZ - hop],
-            dn_send.at[hop],
-            dn_recv.at[hop],
+            tok.at[hop - 1, part],
+            tok.at[hop, part],
+            up_send.at[chunk, hop],
+            up_recv.at[chunk, hop],
+            above,
+        )
+
+    def ag_down(hop, chunk):
+        part = pl.ds(chunk * part_tok, part_tok)
+        return remote(
+            tok.at[lax.rem(NZ + 1 - hop, NZ), part],
+            tok.at[NZ - hop, part],
+            dn_send.at[chunk, hop],
+            dn_recv.at[chunk, hop],
             below,
         )
-
-    half_tok = tokens // 2
-
-    def last_up():
-        part = pl.ds(0, half_tok)
-        return remote(tok.at[3, part], tok.at[4, part], up_send.at[4], up_recv.at[4], above)
-
-    def last_down():
-        part = pl.ds(half_tok, half_tok)
-        return remote(tok.at[5, part], tok.at[4, part], dn_send.at[4], dn_recv.at[4], below)
 
     def slot_copy(j):
         peer = (ep, lax.rem(z + j, NZ) * 2 + core)
         return remote(slots.at[0], slots.at[j], slot_send.at[j], slot_recv.at[j], peer)
 
-    ag_up(1).start()
-    ag_down(1).start()
-
     def send_slots(j, _):
         slot_copy(j).start()
         return 0
 
     lax.fori_loop(1, NZ, send_slots, 0)
+    for chunk in range(2):
+        ag_up(1, chunk).start()
+        ag_down(1, chunk).start()
 
     def kv_copy(source, target):
         return remote(
@@ -225,7 +231,7 @@
             peer = lax.rem(ep + j, EP)
             remote(
                 outgoing.at[step, peer],
-                arrived.at[step, ep],
+                arrived.at[step, position_here],
                 disp_send.at[step],
                 disp_recv.at[step],
                 (peer, tp),
@@ -233,49 +239,48 @@
             return 0
 
         lax.fori_loop(1, EP, send, 0)
-        arrived[step, ep] = outgoing[step, ep]
+        arrived[step, position_here] = outgoing[step, ep]
 
     def all_but_one(buffer, send, recv):
         block = buffer.at[pl.ds(0, EP - 1)]
         return remote(block, block, send, recv, sibling)
 
-    dispatch(0, 0)
-
     def wait_slots(j, _):
         slot_copy(j).wait_recv()
         return 0
-
-    lax.fori_loop(1, NZ, wait_slots, 0)
 
     def advance(step):
         @pl.when(step <= 3)
         def _():
-            ag_up(step).wait_recv()
-
-            @pl.when(step <= 2)
-            def _():
-                ag_up(step + 1).start()
-
-            @pl.when(step == 3)
-            def _():
-                last_up().start()
-
-            ag_down(step).wait_recv()
-
-            @pl.when(step <= 2)
-            def _():
-                ag_down(step + 1).start()
-
-            @pl.when(step == 3)
-            def _():
-                last_down().start()
+            for chunk in range(2):
+                with jax.named_scope("wait_up"):
+                    ag_up(step, chunk).wait_recv()
+
+                @pl.when(step <= 3 - chunk)
+                def _():
+                    ag_up(step + 1, chunk).start()
+
+                with jax.named_scope("wait_down"):
+                    ag_down(step, chunk).wait_recv()
+
+                @pl.when(step <= 2 + chunk)
+                def _():
+                    ag_down(step + 1, chunk).start()
 
         @pl.when(step == 4)
         def _():
-            last_up().wait_recv()
-            last_down().wait_recv()
-
-        dispatch(step, jnp.where(ep < HALF, step, NZ - step))
+            with jax.named_scope("wait_last"):
+                ag_up(4, 0).wait_recv()
+                ag_down(4, 1).wait_recv()
+
+        @pl.when(step == 1)
+        def _():
+            with jax.named_scope("wait_slots"):
+                lax.fori_loop(1, NZ, wait_slots, 0)
+
+        with jax.named_scope("dispatch"):
+            distance = lax.rem(jnp.where(goes_up, step, NZ - step), NZ)
+            dispatch(lax.rem(step, NZ), distance)
 
     def attention():
         query_norm = norm_heads(query_ref[...], query_gain_ref[...])
@@ -356,91 +361,107 @@
 
     def experts(step):
         rows_in = arrived[lax.rem(step, NZ)].reshape(EP * CAP, width)
-        total = None
-        for i in range(2):
-            gate = jnp.dot(rows_in, gate_w[i], preferred_element_type=F32)
-            up = jnp.dot(rows_in, up_w[i], preferred_element_type=F32)
-            hidden = (gate / (1.0 + jnp.exp(-gate)) * up).astype(BF16)
-            term = jnp.dot(hidden, down_w[i], preferred_element_type=F32)
-            total = term if total is None else total + term
-        terms[...] = total
-
-    def ring(step, part, device):
+        across = (((1,), (1,)), ((), ()))
+        units = 2 * gate_w.shape[1]
+        gate = lax.dot_general(
+            rows_in, gate_w[...].reshape(units, width), across, preferred_element_type=F32
+        )
+        up = lax.dot_general(
+            rows_in, up_w[...].reshape(units, width), across, preferred_element_type=F32
+        )
+        hidden = (gate / (1.0 + jnp.exp(-gate)) * up).astype(BF16)
+        terms[...] = jnp.dot(
+            hidden, down_w[...].reshape(units, width), preferred_element_type=F32
+        )
+
+    quarter = EP // 4
+    quarter_rows = quarter * CAP
+
+    def ring(step, part, chunk):
+        blocks = pl.ds((part * 2 + chunk) * quarter, quarter)
         return remote(
-            ring_out.at[step, pl.ds(part * HALF, HALF)],
-            ring_in.at[step + 1, pl.ds(part * HALF, HALF)],
-            ring_send.at[part, step],
-            ring_recv.at[part, step + 1],
-            device,
-        )
-
-    half_rows = HALF * CAP
+            ring_out.at[step, blocks],
+            ring_in.at[step + 1, blocks],
+            ring_send.at[part * 2 + chunk, step],
+            ring_recv.at[part * 2 + chunk, step + 1],
+            (above, below)[part],
+        )
 
     def combine(step):
-        for part, device in ((0, above), (1, below)):
-            blocks = pl.ds(part * HALF, HALF)
-            mine = terms[part * half_rows : (part + 1) * half_rows, :]
-
-            @pl.when(step == 1)
-            def _():
-                ring_out[step, blocks] = mine.astype(BF16).reshape(HALF, CAP, width)
-
-            @pl.when(step >= 2)
-            def _():
-                ring(step - 1, part, device).wait_recv()
-                sofar = ring_in[step, blocks].reshape(half_rows, width).astype(F32)
-                ring_out[step, blocks] = (mine + sofar).astype(BF16).reshape(HALF, CAP, width)
-
-            @pl.when(step < NZ)
-            def _():
-                ring(step, part, device).start()
-
-            @pl.when(step == NZ)
-            def _():
-                def send(j, _):
-                    peer = part * HALF + j
-
-                    @pl.when(peer != ep)
-                    def _():
-                        remote(
-                            ring_out.at[NZ, peer],
-                            returned.at[ep],
-                            ret_send,
-                            ret_recv,
-                            (peer, tp),
-                        ).start()
-
-                    return 0
-
-                lax.fori_loop(0, HALF, send, 0)
+        for chunk in range(2):
+            for part in range(2):
+                first = (part * 2 + chunk) * quarter
+                blocks = pl.ds(first, quarter)
+                mine = terms[first * CAP : (first + quarter) * CAP, :]
+
+                @pl.when(step == 1)
+                def _():
+                    ring_out[step, blocks] = mine.astype(BF16).reshape(quarter, CAP, width)
+
+                @pl.when(step >= 2)
+                def _():
+                    with jax.named_scope("wait_ring"):
+                        ring(step - 1, part, chunk).wait_recv()
+                    sofar = ring_in[step, blocks].reshape(quarter_rows, width).astype(F32)
+                    total = (mine + sofar).astype(BF16)
+                    ring_out[step, blocks] = total.reshape(quarter, CAP, width)
+
+                @pl.when(step < NZ)
+                def _():
+                    ring(step, part, chunk).start()
+
+                @pl.when(step == NZ)
+                def _():
+                    def send(j, _):
+                        peer = at_position(first + j)
+
+                        @pl.when(peer != ep)
+                        def _():
+                            remote(
+                                ring_out.at[NZ, first + j],
+                                returned.at[ep],
+                                ret_send,
+                                ret_recv,
+                                (peer, tp),
+                            ).start()
+
+                        return 0
+
+                    lax.fori_loop(0, quarter, send, 0)
 
     advance(1)
-    attention()
+    advance(2)
+    with jax.named_scope("attention"):
+        attention()
     mix_pair().start()
     for i in range(3):
         loads[i].wait()
         pair_copies[i].wait_recv()
 
     def one_step(step, _):
-        @pl.when(step + 1 < NZ)
-        def _():
-            advance(step + 1)
-
         every = all_but_one(
             arrived.at[lax.rem(step, NZ)], disp_send.at[0], disp_recv.at[lax.rem(step, NZ)]
         )
-        every.wait_recv()
-        experts(step)
+        with jax.named_scope("wait_arrived"):
+            every.wait_recv()
+        with jax.named_scope("experts"):
+            experts(step)
+
+        @pl.when(step + 2 <= NZ)
+        def _():
+            advance(step + 2)
+
         combine(step)
 
         @pl.when(step == 1)
         def _():
-            mix_terms()
+            with jax.named_scope("mixer"):
+                mix_terms()
 
         return 0
 
     lax.fori_loop(1, NZ + 1, one_step, 0)
-    returned[ep] = ring_out[NZ, ep]
+    returned[ep] = ring_out[NZ, position_here]
 
     peers = mix_in.at[pl.ds(1, NZ - 1)]
     remote(peers, peers, mix_send, mix_recv, sibling).wait()
@@ -449,23 +470,28 @@
         total = total + mix_in[j].astype(F32)
     attn_out[...] = total.astype(BF16)
 
+    def column(row):
+        return jnp.transpose(jnp.broadcast_to(row, (tokens, tokens)))[:, 0:1]
+
     slot_lane = iota((tokens, EP * CAP), 1).astype(F32)
-    select_a = jnp.where(slot_lane == slot_a, 1.0, 0.0).astype(BF16)
-    select_b = jnp.where(slot_lane == slot_b, 1.0, 0.0).astype(BF16)
-    score_a, score_b = scores_ref[:, 0:1], scores_ref[:, 1:2]
-    weight_a = 1.0 / (1.0 + jnp.exp(score_b - score_a))
-    weight_b = 1.0 / (jnp.exp(score_a - score_b) + 1.0)
-    all_but_one(returned, ret_send, ret_recv).wait()
+    select_a = jnp.where(slot_lane == column(slots[0, 0][0:1]), 1.0, 0.0).astype(BF16)
+    select_b = jnp.where(slot_lane == column(slots[0, 1][0:1]), 1.0, 0.0).astype(BF16)
+    score_a, score_b = scores_ref[0:1, :], scores_ref[1:2, :]
+    weight_a = column(1.0 / (1.0 + jnp.exp(score_b - score_a)))
+    weight_b = column(1.0 / (jnp.exp(score_a - score_b) + 1.0))
+    with jax.named_scope("wait_returned"):
+        all_but_one(returned, ret_send, ret_recv).wait()
     results = returned[...].reshape(EP * CAP, width)
     result_a = jnp.dot(select_a, results, preferred_element_type=F32)
     result_b = jnp.dot(select_b, results, preferred_element_type=F32)
     expert_out[...] = (weight_a * result_a + weight_b * result_b).astype(BF16)
 
     for hop in range(1, 4):
-        ag_up(hop).wait_send()
-        ag_down(hop).wait_send()
-    last_up().wait_send()
-    last_down().wait_send()
+        for chunk in range(2):
+            ag_up(hop, chunk).wait_send()
+            ag_down(hop, chunk).wait_send()
+    ag_up(4, 0).wait_send()
+    ag_down(4, 1).wait_send()
     mix_pair().wait_send()
     for copy in pair_copies:
         copy.wait_send()
@@ -489,8 +515,9 @@
     lax.fori_loop(0, NZ, drain_dispatch, 0)
 
     def drain_ring(step, _):
-        ring(step, 0, above).wait_send()
-        ring(step, 1, below).wait_send()
+        for chunk in range(2):
+            for part in range(2):
+                ring(step, part, chunk).wait_send()
         return 0
 
     lax.fori_loop(1, NZ, drain_ring, 0)
@@ -528,8 +555,8 @@
         in_specs=[vmem] * 5 + [smem, hbm] + [vmem] * 4 + [hbm] * 3,
         out_specs=(vmem, vmem),
         scratch_shapes=[
-            pltpu.VMEM((2, width, units), BF16),
-            pltpu.VMEM((2, width, units), BF16),
+            pltpu.VMEM((2, units, width), BF16),
+            pltpu.VMEM((2, units, width), BF16),
             pltpu.VMEM((2, units, width), BF16),
             pltpu.VMEM((2, 128, width), BF16),
             pltpu.VMEM((EP, 2, rows, 128), BF16),
@@ -550,16 +577,16 @@
             dma((5,)),
             dma((EP,)),
             dma((EP,)),
-            dma((5,)),
-            dma((5,)),
-            dma((5,)),
-            dma((5,)),
+            dma((2, 5)),
+            dma((2, 5)),
+            dma((2, 5)),
+            dma((2, 5)),
             dma((NZ,)),
             dma((NZ,)),
             dma((NZ,)),
             dma((NZ,)),
-            dma((2, NZ + 1)),
-            dma((2, NZ + 1)),
+            dma((4, NZ + 1)),
+            dma((4, NZ + 1)),
             dma,
             dma,
             dma,
@@ -572,16 +599,16 @@
         query_rows,
         key_rows,
         value_rows,
-        jnp.tile(query_norm_gain, 2)[None, :],
-        jnp.tile(key_gain, 2)[None, :],
+        query_norm_gain[None, :],
+        key_gain[None, :],
         break_offset,
         mixer_out_weight,
         routed_tokens,
         expert_gain[None, :],
-        routes,
-        route_scores,
-        gate_weight[0],
-        up_weight[0],
+        routes.T,
+        route_scores.T,
+        gate_weight[0].T,
+        up_weight[0].T,
         down_weight[0],
     )
 

time: 179 us -> 159 us (0.89)
  Pallas kernels: 166 us -> 154 us
  local copies, waits for them, and re-layouts: 10.3 us -> 3.26 us
    pallas_call x1, Pallas kernels: 166 us -> 154 us  [body(): pl.pallas_call(kernel, out_shape=(jax.ShapeDtypeStruct((rows // (2 * NZ),...]
    unnamed x16 -> x2, local copies, waits for them, and re-layouts: 9.12 us -> 3.26 us
where the time goes in v2:
time: 159 us; the launch traced here: 158 us
  Pallas kernels  154 us (97%)
  local copies, waits for them, and re-layouts  3.26 us (2%)
    pallas_call x1, Pallas kernels, body(): pl.pallas_call(kernel, out_shape=(jax.ShapeDtypeStruct((rows // (2 * NZ),...  154 us
    unnamed x2, local copies, waits for them, and re-layouts  3.26 us

profile of v2, /device:TPU:6, one launch (start us, length us, event | category | flops | bytes accessed | tf_op | source)
XLA Modules:
  0.0 158.3 jit_solution(16845341142762500630)
XLA Ops:
  0.6 154.4 %shard_map.149 = (bf16[8,2048]{1,0:T(8,128)(2,1)}, bf16[128,2048]{1,0:T(8,128)(2,1)}) custom-call(bf16[128,128]{1,0:T(8,128)(2,1)} %query_ref.1, bf16[128,128]{1,0:T(8,128)(2,1)} %key_ref.1, bf16[128,128]{1,0:T(8,128)(2,1)} %value_ref.1, f32[1,64]{1,0:T(1,128)} %bitcast.18, f32[1,64]{1,0:T(1,128)} %bitcast.19, f32[2]{0:T(128)} %offset_ref.1, ...), custom_call_target="tpu_custom_call" | custom-call | tf_op jit(solution)/shard_map/pallas_call | solution.py:549
  155.0 1.4 copy.18
  156.4 1.9 %copy.19 = bf16[128,2048]{1,0:T(8,128)(2,1)} copy(bf16[128,2048]{1,0:T(8,128)(2,1)} %get-tuple-element.5) | data formatting | bytes 1048576

commit v3 on v2

--- a/solution.py
+++ b/solution.py
@@ -14,6 +14,8 @@
 NZ = 8
 CAP = 16
 HALF = EP // 2
+PIECES = 2
+CHUNKS = 4
 F32 = jnp.float32
 BF16 = jnp.bfloat16
 
@@ -23,22 +25,33 @@
 
 
 def kernel(
+    query_hbm,
+    key_hbm,
+    value_hbm,
+    query_gain_hbm,
+    key_gain_hbm,
+    offset_hbm,
+    mixer_hbm,
+    tokens_hbm,
+    expert_gain_hbm,
+    routes_hbm,
+    scores_hbm,
+    gate_hbm,
+    up_hbm,
+    down_hbm,
+    attn_hbm,
+    blend_hbm,
+    returned,
     query_ref,
     key_ref,
     value_ref,
     query_gain_ref,
     key_gain_ref,
     offset_ref,
-    mixer_hbm,
     tokens_ref,
     expert_gain_ref,
     routes_ref,
     scores_ref,
-    gate_hbm,
-    up_hbm,
-    down_hbm,
-    attn_out,
-    expert_out,
     gate_w,
     up_w,
     down_w,
@@ -51,12 +64,14 @@
     terms,
     ring_out,
     ring_in,
-    returned,
+    blend,
     mix_mine,
     mix_theirs,
+    mix_terms,
     mix_out,
     mix_in,
     load_sem,
+    small_sem,
     pair_send,
     pair_recv,
     kv_send,
@@ -82,8 +97,8 @@
     above = (ep, lax.rem(z + 1, NZ) * 2 + core)
     below = (ep, lax.rem(z + NZ - 1, NZ) * 2 + core)
     sibling = (ep, z * 2 + 1 - core)
-    rows = query_ref.shape[0]
-    tokens, width = tokens_ref.shape
+    rows = query_hbm.shape[0]
+    tokens, width = tokens_hbm.shape
     position_here = lax.rem(ep // 4 + ep % 4, 4) * 4 + ep // 4
     goes_up = position_here < HALF
 
@@ -102,24 +117,28 @@
 
     barrier = pltpu.get_barrier_semaphore()
 
-    def greet_ep(j, _):
-        pl.semaphore_signal(
-            barrier, inc=1, device_id=(lax.rem(ep + j, EP), tp), device_id_type=MESH
-        )
-        return 0
-
-    def greet_z(j, _):
-        pl.semaphore_signal(
-            barrier,
-            inc=1,
-            device_id=(ep, lax.rem(z + j, NZ) * 2 + core),
-            device_id_type=MESH,
-        )
-        return 0
-
-    lax.fori_loop(1, EP, greet_ep, 0)
-    lax.fori_loop(1, NZ, greet_z, 0)
-    pl.semaphore_signal(barrier, inc=1, device_id=sibling, device_id_type=MESH)
+    greeted = [(ep, lax.rem(z + j, NZ) * 2 + core) for j in range(1, NZ)]
+    greeted += [(lax.rem(ep + j, EP), tp) for j in range(1, EP)] + [sibling]
+    for peer in greeted:
+        pl.semaphore_signal(barrier, inc=1, device_id=peer, device_id_type=MESH)
+
+    operands = (
+        (tokens_hbm, tokens_ref),
+        (expert_gain_hbm, expert_gain_ref),
+        (routes_hbm, routes_ref),
+        (key_hbm, key_ref),
+        (value_hbm, value_ref),
+        (key_gain_hbm, key_gain_ref),
+        (query_hbm, query_ref),
+        (query_gain_hbm, query_gain_ref),
+        (offset_hbm, offset_ref),
+        (scores_hbm, scores_ref),
+    )
+    small = [
+        pltpu.make_async_copy(src, dst, small_sem.at[i]) for i, (src, dst) in enumerate(operands)
+    ]
+    for copy in small:
+        copy.start()
 
     weights = ((gate_hbm, gate_w), (up_hbm, up_w), (down_hbm, down_w), (mixer_hbm, mixer_w))
     loads = [
@@ -140,10 +159,8 @@
         scale = jnp.where(first_head, lax.rsqrt(mean_a + EPS), lax.rsqrt(mean_b + EPS))
         return (split * scale * jnp.concatenate([gain, gain], axis=1)).astype(BF16)
 
-    key_norm = norm_heads(key_ref[...], key_gain_ref[...])
-    kv[ep, 0] = key_norm
-    kv[ep, 1] = value_ref[...]
-
+    for copy in small[:3]:
+        copy.wait()
     as_float = tokens_ref[...].astype(F32)
     mean = jnp.mean(as_float * as_float, axis=1, keepdims=True)
     tok[0] = (as_float * lax.rsqrt(mean + EPS) * expert_gain_ref[...]).astype(BF16)
@@ -162,8 +179,14 @@
     slots[0, 0] = jnp.broadcast_to(slot_a, (8, tokens))
     slots[0, 1] = jnp.broadcast_to(slot_b, (8, tokens))
 
+    for copy in small[3:]:
+        copy.wait()
+    key_norm = norm_heads(key_ref[...], key_gain_ref[...])
+    kv[ep, 0] = key_norm
+    kv[ep, 1] = value_ref[...]
+
     with jax.named_scope("wait_entry"):
-        pl.semaphore_wait(barrier, EP - 1 + NZ - 1 + 1)
+        pl.semaphore_wait(barrier, len(greeted))
 
     part_tok = tokens // 2
 
@@ -189,7 +212,7 @@
 
     def slot_copy(j):
         peer = (ep, lax.rem(z + j, NZ) * 2 + core)
-        return remote(slots.at[0], slots.at[j], slot_send.at[j], slot_recv.at[j], peer)
+        return remote(slots.at[0], slots.at[j], slot_send, slot_recv.at[j], peer)
 
     def send_slots(j, _):
         slot_copy(j).start()
@@ -198,7 +221,7 @@
     lax.fori_loop(1, NZ, send_slots, 0)
     for chunk in range(2):
         ag_up(1, chunk).start()
-        ag_down(1, chunk).start()
+        ag_down(1, 1 - chunk).start()
 
     def kv_copy(source, target):
         return remote(
@@ -225,21 +248,21 @@
         row_b = slots[distance, 1][0:1]
         pick = jnp.where((slot_rows == row_a) | (slot_rows == row_b), 1.0, 0.0).astype(BF16)
         picked = jnp.dot(pick, tok[distance], preferred_element_type=F32).astype(BF16)
-        outgoing[step] = picked.reshape(EP, CAP, width)
+        outgoing[pl.ds(step * EP, EP)] = picked.reshape(EP, CAP, width)
 
         def send(j, _):
             peer = lax.rem(ep + j, EP)
             remote(
-                outgoing.at[step, peer],
+                outgoing.at[step * EP + peer],
                 arrived.at[step, position_here],
-                disp_send.at[step],
+                disp_send,
                 disp_recv.at[step],
                 (peer, tp),
             ).start()
             return 0
 
         lax.fori_loop(1, EP, send, 0)
-        arrived[step, position_here] = outgoing[step, ep]
+        arrived[step, position_here] = outgoing[step * EP + ep]
 
     def all_but_one(buffer, send, recv):
         block = buffer.at[pl.ds(0, EP - 1)]
@@ -261,11 +284,11 @@
                     ag_up(step + 1, chunk).start()
 
                 with jax.named_scope("wait_down"):
-                    ag_down(step, chunk).wait_recv()
-
-                @pl.when(step <= 2 + chunk)
+                    ag_down(step, 1 - chunk).wait_recv()
+
+                @pl.when(step <= 3 - chunk)
                 def _():
-                    ag_down(step + 1, chunk).start()
+                    ag_down(step + 1, 1 - chunk).start()
 
         @pl.when(step == 4)
         def _():
@@ -343,21 +366,43 @@
             mix_mine.at[1 - core], mix_theirs, pair_send.at[4], pair_recv.at[4], sibling
         )
 
-    def mix_terms():
+    def project():
         loads[3].wait()
         pair_copies[3].wait_recv()
         mix_pair().wait_recv()
         term = jnp.dot(mix_mine[core], mixer_w[0], preferred_element_type=F32)
         term = term + jnp.dot(mix_theirs[...], mixer_w[1], preferred_element_type=F32)
         for i in range(NZ):
-            mix_out[i] = term[8 * i : 8 * i + 8].astype(BF16)
-
-        def send(j, _):
-            to = lax.rem(z + j, NZ)
-            remote(mix_out.at[to], mix_in.at[j], mix_send, mix_recv, (ep, to * 2 + core)).start()
-            return 0
-
-        lax.fori_loop(1, NZ, send, 0)
+            for part in range(2):
+                columns = slice(part * width // 2, (part + 1) * width // 2)
+                mix_terms[i, part] = term[8 * i : 8 * i + 8, columns]
+
+    def mix_ring(step, part):
+        return remote(
+            mix_out.at[step, part],
+            mix_in.at[step + 1, part],
+            mix_send,
+            mix_recv.at[part, step + 1],
+            (above, below)[part],
+        )
+
+    def mix(step):
+        for part, owner in ((0, z + NZ - step), (1, z + step)):
+            mine = mix_terms[lax.rem(owner, NZ), part]
+
+            @pl.when(step == 1)
+            def _():
+                mix_out[step, part] = mine.astype(BF16)
+
+            @pl.when(step >= 2)
+            def _():
+                with jax.named_scope("wait_mix"):
+                    mix_ring(step - 1, part).wait_recv()
+                mix_out[step, part] = (mine + mix_in[step, part].astype(F32)).astype(BF16)
+
+            @pl.when(step < NZ)
+            def _():
+                mix_ring(step, part).start()
 
     def experts(step):
         rows_in = arrived[lax.rem(step, NZ)].reshape(EP * CAP, width)
@@ -374,37 +419,37 @@
             hidden, down_w[...].reshape(units, width), preferred_element_type=F32
         )
 
-    quarter = EP // 4
-    quarter_rows = quarter * CAP
+    share = EP // (2 * CHUNKS)
+    share_rows = share * CAP
 
     def ring(step, part, chunk):
-        blocks = pl.ds((part * 2 + chunk) * quarter, quarter)
+        blocks = pl.ds((part * CHUNKS + chunk) * share, share)
         return remote(
             ring_out.at[step, blocks],
             ring_in.at[step + 1, blocks],
-            ring_send.at[part * 2 + chunk, step],
-            ring_recv.at[part * 2 + chunk, step + 1],
+            ring_send,
+            ring_recv.at[part * CHUNKS + chunk, step + 1],
             (above, below)[part],
         )
 
     def combine(step):
-        for chunk in range(2):
+        for chunk in range(CHUNKS):
             for part in range(2):
-                first = (part * 2 + chunk) * quarter
-                blocks = pl.ds(first, quarter)
-                mine = terms[first * CAP : (first + quarter) * CAP, :]
+                first = (part * CHUNKS + chunk) * share
+                blocks = pl.ds(first, share)
+                mine = terms[first * CAP : (first + share) * CAP, :]
 
                 @pl.when(step == 1)
                 def _():
-                    ring_out[step, blocks] = mine.astype(BF16).reshape(quarter, CAP, width)
+                    ring_out[step, blocks] = mine.astype(BF16).reshape(share, CAP, width)
 
                 @pl.when(step >= 2)
                 def _():
                     with jax.named_scope("wait_ring"):
                         ring(step - 1, part, chunk).wait_recv()
-                    sofar = ring_in[step, blocks].reshape(quarter_rows, width).astype(F32)
+                    sofar = ring_in[step, blocks].reshape(share_rows, width).astype(F32)
                     total = (mine + sofar).astype(BF16)
-                    ring_out[step, blocks] = total.reshape(quarter, CAP, width)
+                    ring_out[step, blocks] = total.reshape(share, CAP, width)
 
                 @pl.when(step < NZ)
                 def _():
@@ -427,7 +472,7 @@
 
                         return 0
 
-                    lax.fori_loop(0, quarter, send, 0)
+                    lax.fori_loop(0, share, send, 0)
 
     advance(1)
     advance(2)
@@ -440,51 +485,52 @@
 
     def one_step(step, _):
         every = all_but_one(
-            arrived.at[lax.rem(step, NZ)], disp_send.at[0], disp_recv.at[lax.rem(step, NZ)]
+            arrived.at[lax.rem(step, NZ)], disp_send, disp_recv.at[lax.rem(step, NZ)]
         )
         with jax.named_scope("wait_arrived"):
             every.wait_recv()
         with jax.named_scope("experts"):
             experts(step)
 
-        @pl.when(step + 2 <= NZ)
+        @pl.when(step <= 2)
         def _():
             advance(step + 2)
 
         combine(step)
+
+        @pl.when((step >= 2) & (step + 3 <= NZ))
+        def _():
+            advance(step + 3)
 
         @pl.when(step == 1)
         def _():
             with jax.named_scope("mixer"):
-                mix_terms()
+                project()
+
+        mix(step)
 
         return 0
 
     lax.fori_loop(1, NZ + 1, one_step, 0)
-    returned[ep] = ring_out[NZ, position_here]
-
-    peers = mix_in.at[pl.ds(1, NZ - 1)]
-    remote(peers, peers, mix_send, mix_recv, sibling).wait()
-    total = mix_out[z].astype(F32)
-    for j in range(1, NZ):
-        total = total + mix_in[j].astype(F32)
-    attn_out[...] = total.astype(BF16)
+    own = pltpu.make_async_copy(ring_out.at[NZ, position_here], returned.at[ep], load_sem.at[4])
+    own.start()
+    attn_copy = pltpu.make_async_copy(mix_out.at[NZ], attn_hbm, load_sem.at[6])
+    attn_copy.start()
 
     def column(row):
         return jnp.transpose(jnp.broadcast_to(row, (tokens, tokens)))[:, 0:1]
 
     slot_lane = iota((tokens, EP * CAP), 1).astype(F32)
-    select_a = jnp.where(slot_lane == column(slots[0, 0][0:1]), 1.0, 0.0).astype(BF16)
-    select_b = jnp.where(slot_lane == column(slots[0, 1][0:1]), 1.0, 0.0).astype(BF16)
     score_a, score_b = scores_ref[0:1, :], scores_ref[1:2, :]
     weight_a = column(1.0 / (1.0 + jnp.exp(score_b - score_a)))
     weight_b = column(1.0 / (jnp.exp(score_a - score_b) + 1.0))
-    with jax.named_scope("wait_returned"):
-        all_but_one(returned, ret_send, ret_recv).wait()
-    results = returned[...].reshape(EP * CAP, width)
-    result_a = jnp.dot(select_a, results, preferred_element_type=F32)
-    result_b = jnp.dot(select_b, results, preferred_element_type=F32)
-    expert_out[...] = (weight_a * result_a + weight_b * result_b).astype(BF16)
+    weight = jnp.where(slot_lane == column(slots[0, 0][0:1]), weight_a, 0.0)
+    weight = jnp.where(slot_lane == column(slots[0, 1][0:1]), weight_b, weight)
+    high = weight.astype(BF16)
+    blend[0] = high
+    blend[1] = (weight - high.astype(F32)).astype(BF16)
+    blend_copy = pltpu.make_async_copy(blend, blend_hbm, load_sem.at[5])
+    blend_copy.start()
 
     for hop in range(1, 4):
         for chunk in range(2):
@@ -496,11 +542,13 @@
     for copy in pair_copies:
         copy.wait_send()
 
-    def drain_slots(j, _):
-        slot_copy(j).wait_send()
-        return 0
-
-    lax.fori_loop(1, NZ, drain_slots, 0)
+    def drain(block, send, recv):
+        remote(block, block, send, recv, sibling).wait_send()
+
+    drain(slots.at[pl.ds(1, NZ - 1)], slot_send, slot_recv.at[0])
+    drain(outgoing.at[pl.ds(0, NZ * (EP - 1))], disp_send, disp_recv.at[0])
+    drain(mix_out.at[pl.ds(1, NZ - 1)], mix_send, mix_recv.at[0, 0])
+    drain(ring_out.at[pl.ds(1, NZ - 1)], ring_send, ring_recv.at[0, 0])
 
     def drain_kv(j, _):
         kv_copy(ep, j).wait_send()
@@ -508,19 +556,25 @@
 
     lax.fori_loop(ep + 1, EP, drain_kv, 0)
 
-    def drain_dispatch(step, _):
-        all_but_one(outgoing.at[step], disp_send.at[step], disp_recv.at[step]).wait_send()
-        return 0
-
-    lax.fori_loop(0, NZ, drain_dispatch, 0)
-
-    def drain_ring(step, _):
-        for chunk in range(2):
-            for part in range(2):
-                ring(step, part, chunk).wait_send()
-        return 0
-
-    lax.fori_loop(1, NZ, drain_ring, 0)
+    with jax.named_scope("wait_returned"):
+        own.wait()
+        blend_copy.wait()
+        all_but_one(returned, ret_send, ret_recv).wait()
+        attn_copy.wait()
+
+
+def blend_kernel(blend_ref, results_ref, attn_ref, expert_out, attn_out):
+    _, tokens, slots = blend_ref.shape
+    parts = jnp.dot(
+        blend_ref[...].reshape(2 * tokens, slots), results_ref[...], preferred_element_type=F32
+    )
+    expert_out[...] = (parts[:tokens] + parts[tokens:]).astype(BF16)
+
+    @pl.when(pl.program_id(0) == 0)
+    def _():
+        half = attn_ref.shape[2]
+        attn_out[:, :half] = attn_ref[0]
+        attn_out[:, half:] = attn_ref[1]
 
 
 def body(
@@ -542,19 +596,28 @@
     rows = query_rows.shape[0]
     tokens, width = routed_tokens.shape
     units = gate_weight.shape[2]
-    vmem = pl.BlockSpec(memory_space=pltpu.VMEM)
-    smem = pl.BlockSpec(memory_space=pltpu.SMEM)
     hbm = pl.BlockSpec(memory_space=pl.ANY)
     dma = pltpu.SemaphoreType.DMA
-    return pl.pallas_call(
+    attn, blend, returned = pl.pallas_call(
         kernel,
         out_shape=(
-            jax.ShapeDtypeStruct((rows // (2 * NZ), width), BF16),
-            jax.ShapeDtypeStruct((tokens, width), BF16),
+            jax.ShapeDtypeStruct((2, rows // (2 * NZ), width // 2), BF16),
+            jax.ShapeDtypeStruct((2, tokens, EP * CAP), BF16),
+            jax.ShapeDtypeStruct((EP, CAP, width), BF16),
         ),
-        in_specs=[vmem] * 5 + [smem, hbm] + [vmem] * 4 + [hbm] * 3,
-        out_specs=(vmem, vmem),
+        in_specs=[hbm] * 14,
+        out_specs=(hbm, hbm, hbm),
         scratch_shapes=[
+            pltpu.VMEM((rows, 128), BF16),
+            pltpu.VMEM((rows, 128), BF16),
+            pltpu.VMEM((rows, 128), BF16),
+            pltpu.VMEM((1, HEAD_DIM), F32),
+            pltpu.VMEM((1, HEAD_DIM), F32),
+            pltpu.SMEM((2,), F32),
+            pltpu.VMEM((tokens, width), BF16),
+            pltpu.VMEM((1, width), F32),
+            pltpu.VMEM((2, tokens), jnp.int32),
+            pltpu.VMEM((2, tokens), F32),
             pltpu.VMEM((2, units, width), BF16),
             pltpu.VMEM((2, units, width), BF16),
             pltpu.VMEM((2, units, width), BF16),
@@ -562,17 +625,19 @@
             pltpu.VMEM((EP, 2, rows, 128), BF16),
             pltpu.VMEM((NZ, tokens, width), BF16),
             pltpu.VMEM((NZ, 2, 8, 128), F32),
-            pltpu.VMEM((NZ, EP, CAP, width), BF16),
+            pltpu.VMEM((NZ * EP, CAP, width), BF16),
             pltpu.VMEM((NZ, EP, CAP, width), BF16),
             pltpu.VMEM((EP * CAP, width), F32),
             pltpu.VMEM((NZ + 1, EP, CAP, width), BF16),
             pltpu.VMEM((NZ + 1, EP, CAP, width), BF16),
-            pltpu.VMEM((EP, CAP, width), BF16),
+            pltpu.VMEM((2, tokens, EP * CAP), BF16),
             pltpu.VMEM((2, 64, 128), BF16),
             pltpu.VMEM((64, 128), BF16),
-            pltpu.VMEM((NZ, 8, width), BF16),
-            pltpu.VMEM((NZ, 8, width), BF16),
-            dma((4,)),
+            pltpu.VMEM((NZ, 2, 8, width // 2), F32),
+            pltpu.VMEM((NZ + 1, 2, 8, width // 2), BF16),
+            pltpu.VMEM((NZ + 1, 2, 8, width // 2), BF16),
+            dma((7,)),
+            dma((10,)),
             dma((5,)),
             dma((5,)),
             dma((EP,)),
@@ -581,16 +646,16 @@
             dma((2, 5)),
             dma((2, 5)),
             dma((2, 5)),
+            dma,
             dma((NZ,)),
+            dma,
             dma((NZ,)),
-            dma((NZ,)),
-            dma((NZ,)),
-            dma((4, NZ + 1)),
-            dma((4, NZ + 1)),
+            dma,
+            dma((2 * CHUNKS, NZ + 1)),
             dma,
             dma,
             dma,
-            dma,
+            dma((2, NZ + 1)),
         ],
         compiler_params=pltpu.CompilerParams(
             collective_id=0, has_side_effects=True, vmem_limit_bytes=67043328
@@ -611,6 +676,25 @@
         up_weight[0].T,
         down_weight[0],
     )
+    piece = width // PIECES
+    expert_output, attention_output = pl.pallas_call(
+        blend_kernel,
+        grid=(PIECES,),
+        out_shape=(
+            jax.ShapeDtypeStruct((tokens, width), BF16),
+            jax.ShapeDtypeStruct((rows // (2 * NZ), width), BF16),
+        ),
+        in_specs=[
+            pl.BlockSpec(blend.shape, lambda i: (0, 0, 0)),
+            pl.BlockSpec((EP * CAP, piece), lambda i: (0, i)),
+            pl.BlockSpec(attn.shape, lambda i: (0, 0, 0)),
+        ],
+        out_specs=(
+            pl.BlockSpec((tokens, piece), lambda i: (0, i)),
+            pl.BlockSpec((rows // (2 * NZ), width), lambda i: (0, 0)),
+        ),
+    )(blend, returned.reshape(EP * CAP, width), attn)
+    return attention_output, expert_output
 
 
 def solution(mesh):

time: 159 us -> 150 us (0.943); the launches traced: 158 us -> 148 us
  Pallas kernels: 154 us -> 147 us
  local copies, waits for them, and re-layouts: 3.26 us -> 0 us
    pallas_call x1 -> x2, Pallas kernels: 154 us -> 147 us  [the longest x1 144 us: body(): pl.pallas_call(kernel, out_shape=(jax.ShapeDtypeStruct((2, rows // (2 * N...]
    unnamed x2 -> x0, local copies, waits for them, and re-layouts: 3.26 us -> none
where the time goes in v3:
time: 150 us; the launch traced here: 148 us
  Pallas kernels  147 us (98%)
    pallas_call x1, Pallas kernels, body(): pl.pallas_call(kernel, out_shape=(jax.ShapeDtypeStruct((2, rows // (2 * N...  144 us

profile of v3, /device:TPU:6, one launch (start us, length us, event | category | flops | bytes accessed | tf_op | source)
XLA Modules:
  0.0 147.5 jit_solution(11726250004426418174)
XLA Ops:
  0.6 144.5 %shard_map.149 = (bf16[2,8,1024]{2,1,0:T(8,128)(2,1)}, bf16[2,128,256]{2,1,0:T(8,128)(2,1)}, bf16[16,16,2048]{2,1,0:T(8,128)(2,1)}) custom-call(bf16[128,128]{1,0:T(8,128)(2,1)} %query_hbm.1, bf16[128,128]{1,0:T(8,128)(2,1)} %key_hbm.1, bf16[128,128]{1,0:T(8,128)(2,1)} %value_hbm.1, f32[1,64]{1,0:T(1,128)} %bitcast.20, f32[1,64]{1,0:T(1,128)} %bitcast.21, ...), custom_call_target="tpu_custom_call" | custom-call | tf_op jit(solution)/shard_map/pallas_call | solution.py:601
  145.1 2.4 %shard_map.150 = (bf16[128,2048]{1,0:T(8,128)(2,1)}, bf16[8,2048]{1,0:T(8,128)(2,1)}) custom-call(bf16[2,128,256]{2,1,0:T(8,128)(2,1)} %get-tuple-element.7.blend_ref, bf16[256,2048]{1,0:T(8,128)(2,1)} %bitcast.13, bf16[2,8,1024]{2,1,0:T(8,128)(2,1)} %get-tuple-element.9.attn_ref), custom_call_target="tpu_custom_call" | custom-call | tf_op jit(solution)/shard_map/pallas_call | solution.py:680

commit v4 on v3

--- a/solution.py
+++ b/solution.py
@@ -76,9 +76,8 @@
     pair_recv,
     kv_send,
     kv_recv,
-    up_send,
+    ag_send,
     up_recv,
-    dn_send,
     dn_recv,
     slot_send,
     slot_recv,
@@ -179,49 +178,49 @@
     slots[0, 0] = jnp.broadcast_to(slot_a, (8, tokens))
     slots[0, 1] = jnp.broadcast_to(slot_b, (8, tokens))
 
+    with jax.named_scope("wait_entry"):
+        pl.semaphore_wait(barrier, len(greeted))
+
+    part_tok = tokens // 2
+
+    def ag_up(hop, chunk):
+        part = pl.ds(chunk * part_tok, part_tok)
+        return remote(
+            tok.at[hop - 1, part],
+            tok.at[hop, part],
+            ag_send,
+            up_recv.at[chunk, hop],
+            above,
+        )
+
+    def ag_down(hop, chunk):
+        part = pl.ds(chunk * part_tok, part_tok)
+        return remote(
+            tok.at[lax.rem(NZ + 1 - hop, NZ), part],
+            tok.at[NZ - hop, part],
+            ag_send,
+            dn_recv.at[chunk, hop],
+            below,
+        )
+
+    def slot_copy(j):
+        peer = (ep, lax.rem(z + j, NZ) * 2 + core)
+        return remote(slots.at[0], slots.at[j], slot_send, slot_recv.at[j], peer)
+
+    def send_slots(j, _):
+        slot_copy(j).start()
+        return 0
+
+    lax.fori_loop(1, NZ, send_slots, 0)
+    for chunk in range(2):
+        ag_up(1, chunk).start()
+        ag_down(1, 1 - chunk).start()
+
     for copy in small[3:]:
         copy.wait()
     key_norm = norm_heads(key_ref[...], key_gain_ref[...])
     kv[ep, 0] = key_norm
     kv[ep, 1] = value_ref[...]
-
-    with jax.named_scope("wait_entry"):
-        pl.semaphore_wait(barrier, len(greeted))
-
-    part_tok = tokens // 2
-
-    def ag_up(hop, chunk):
-        part = pl.ds(chunk * part_tok, part_tok)
-        return remote(
-            tok.at[hop - 1, part],
-            tok.at[hop, part],
-            up_send.at[chunk, hop],
-            up_recv.at[chunk, hop],
-            above,
-        )
-
-    def ag_down(hop, chunk):
-        part = pl.ds(chunk * part_tok, part_tok)
-        return remote(
-            tok.at[lax.rem(NZ + 1 - hop, NZ), part],
-            tok.at[NZ - hop, part],
-            dn_send.at[chunk, hop],
-            dn_recv.at[chunk, hop],
-            below,
-        )
-
-    def slot_copy(j):
-        peer = (ep, lax.rem(z + j, NZ) * 2 + core)
-        return remote(slots.at[0], slots.at[j], slot_send, slot_recv.at[j], peer)
-
-    def send_slots(j, _):
-        slot_copy(j).start()
-        return 0
-
-    lax.fori_loop(1, NZ, send_slots, 0)
-    for chunk in range(2):
-        ag_up(1, chunk).start()
-        ag_down(1, 1 - chunk).start()
 
     def kv_copy(source, target):
         return remote(
@@ -419,37 +418,36 @@
             hidden, down_w[...].reshape(units, width), preferred_element_type=F32
         )
 
-    share = EP // (2 * CHUNKS)
-    share_rows = share * CAP
+    share = width // CHUNKS
 
     def ring(step, part, chunk):
-        blocks = pl.ds((part * CHUNKS + chunk) * share, share)
+        block = (pl.ds(part * HALF, HALF), slice(None), pl.ds(chunk * share, share))
         return remote(
-            ring_out.at[step, blocks],
-            ring_in.at[step + 1, blocks],
+            ring_out.at[step, *block],
+            ring_in.at[step - 1, *block],
             ring_send,
-            ring_recv.at[part * CHUNKS + chunk, step + 1],
+            ring_recv.at[part * CHUNKS + chunk, step - 1],
             (above, below)[part],
         )
 
     def combine(step):
         for chunk in range(CHUNKS):
+            columns = slice(chunk * share, (chunk + 1) * share)
             for part in range(2):
-                first = (part * CHUNKS + chunk) * share
-                blocks = pl.ds(first, share)
-                mine = terms[first * CAP : (first + share) * CAP, :]
+                blocks = pl.ds(part * HALF, HALF)
+                mine = terms[part * HALF * CAP : (part + 1) * HALF * CAP, columns]
 
                 @pl.when(step == 1)
                 def _():
-                    ring_out[step, blocks] = mine.astype(BF16).reshape(share, CAP, width)
+                    ring_out[step, blocks, :, columns] = mine.astype(BF16).reshape(HALF, CAP, share)
 
                 @pl.when(step >= 2)
                 def _():
                     with jax.named_scope("wait_ring"):
                         ring(step - 1, part, chunk).wait_recv()
-                    sofar = ring_in[step, blocks].reshape(share_rows, width).astype(F32)
-                    total = (mine + sofar).astype(BF16)
-                    ring_out[step, blocks] = total.reshape(share, CAP, width)
+                    sofar = ring_in[step - 2, blocks, :, columns].reshape(HALF * CAP, share)
+                    total = (mine + sofar.astype(F32)).astype(BF16)
+                    ring_out[step, blocks, :, columns] = total.reshape(HALF, CAP, share)
 
                 @pl.when(step < NZ)
                 def _():
@@ -458,13 +456,14 @@
                 @pl.when(step == NZ)
                 def _():
                     def send(j, _):
-                        peer = at_position(first + j)
+                        place = part * HALF + j
+                        peer = at_position(place)
 
                         @pl.when(peer != ep)
                         def _():
                             remote(
-                                ring_out.at[NZ, first + j],
-                                returned.at[ep],
+                                ring_out.at[NZ, place, :, pl.ds(chunk * share, share)],
+                                returned.at[ep, :, pl.ds(chunk * share, share)],
                                 ret_send,
                                 ret_recv,
                                 (peer, tp),
@@ -472,7 +471,7 @@
 
                         return 0
 
-                    lax.fori_loop(0, share, send, 0)
+                    lax.fori_loop(0, HALF, send, 0)
 
     advance(1)
     advance(2)
@@ -532,12 +531,6 @@
     blend_copy = pltpu.make_async_copy(blend, blend_hbm, load_sem.at[5])
     blend_copy.start()
 
-    for hop in range(1, 4):
-        for chunk in range(2):
-            ag_up(hop, chunk).wait_send()
-            ag_down(hop, chunk).wait_send()
-    ag_up(4, 0).wait_send()
-    ag_down(4, 1).wait_send()
     mix_pair().wait_send()
     for copy in pair_copies:
         copy.wait_send()
@@ -545,6 +538,7 @@
     def drain(block, send, recv):
         remote(block, block, send, recv, sibling).wait_send()
 
+    drain(tok.at[pl.ds(0, NZ - 1)], ag_send, up_recv.at[0, 0])
     drain(slots.at[pl.ds(1, NZ - 1)], slot_send, slot_recv.at[0])
     drain(outgoing.at[pl.ds(0, NZ * (EP - 1))], disp_send, disp_recv.at[0])
     drain(mix_out.at[pl.ds(1, NZ - 1)], mix_send, mix_recv.at[0, 0])
@@ -629,7 +623,7 @@
             pltpu.VMEM((NZ, EP, CAP, width), BF16),
             pltpu.VMEM((EP * CAP, width), F32),
             pltpu.VMEM((NZ + 1, EP, CAP, width), BF16),
-            pltpu.VMEM((NZ + 1, EP, CAP, width), BF16),
+            pltpu.VMEM((NZ - 1, EP, CAP, width), BF16),
             pltpu.VMEM((2, tokens, EP * CAP), BF16),
             pltpu.VMEM((2, 64, 128), BF16),
             pltpu.VMEM((64, 128), BF16),
@@ -642,8 +636,7 @@
             dma((5,)),
             dma((EP,)),
             dma((EP,)),
-            dma((2, 5)),
-            dma((2, 5)),
+            dma,
             dma((2, 5)),
             dma((2, 5)),
             dma,
@@ -651,7 +644,7 @@
             dma,
             dma((NZ,)),
             dma,
-            dma((2 * CHUNKS, NZ + 1)),
+            dma((2 * CHUNKS, NZ - 1)),
             dma,
             dma,
             dma,

time: 150 us -> 147 us (0.980)
  Pallas kernels: 147 us -> 145 us
    pallas_call x1, Pallas kernels: 144 us -> 142 us  [body(): pl.pallas_call(kernel, out_shape=(jax.ShapeDtypeStruct((2, rows // (2 * N...]
where the time goes in v4:
time: 147 us; the launch traced here: 145 us
  Pallas kernels  145 us (99%)
    pallas_call x1, Pallas kernels, body(): pl.pallas_call(kernel, out_shape=(jax.ShapeDtypeStruct((2, rows // (2 * N...  142 us

profile of v4, /device:TPU:6, one launch (start us, length us, event | category | flops | bytes accessed | tf_op | source)
XLA Modules:
  0.0 145.2 jit_solution(3265364367918381658)
XLA Ops:
  0.6 142.1 %shard_map.149 = (bf16[2,8,1024]{2,1,0:T(8,128)(2,1)}, bf16[2,128,256]{2,1,0:T(8,128)(2,1)}, bf16[16,16,2048]{2,1,0:T(8,128)(2,1)}) custom-call(bf16[128,128]{1,0:T(8,128)(2,1)} %query_hbm.1, bf16[128,128]{1,0:T(8,128)(2,1)} %key_hbm.1, bf16[128,128]{1,0:T(8,128)(2,1)} %value_hbm.1, f32[1,64]{1,0:T(1,128)} %bitcast.20, f32[1,64]{1,0:T(1,128)} %bitcast.21, ...), custom_call_target="tpu_custom_call" | custom-call | tf_op jit(solution)/shard_map/pallas_call | solution.py:595
  142.7 2.4 %shard_map.150 = (bf16[128,2048]{1,0:T(8,128)(2,1)}, bf16[8,2048]{1,0:T(8,128)(2,1)}) custom-call(bf16[2,128,256]{2,1,0:T(8,128)(2,1)} %get-tuple-element.7.blend_ref, bf16[256,2048]{1,0:T(8,128)(2,1)} %bitcast.13, bf16[2,8,1024]{2,1,0:T(8,128)(2,1)} %get-tuple-element.9.attn_ref), custom_call_target="tpu_custom_call" | custom-call | tf_op jit(solution)/shard_map/pallas_call | solution.py:673

commit v5 on v4

--- a/solution.py
+++ b/solution.py
@@ -15,7 +15,7 @@
 CAP = 16
 HALF = EP // 2
 PIECES = 2
-CHUNKS = 4
+CHUNKS = 8
 F32 = jnp.float32
 BF16 = jnp.bfloat16
 
@@ -250,7 +250,7 @@
         outgoing[pl.ds(step * EP, EP)] = picked.reshape(EP, CAP, width)
 
         def send(j, _):
-            peer = lax.rem(ep + j, EP)
+            peer = lax.rem(ep // 4 + j // 4, 4) * 4 + lax.rem(ep % 4 + j % 4, 4)
             remote(
                 outgoing.at[step * EP + peer],
                 arrived.at[step, position_here],
@@ -456,7 +456,7 @@
                 @pl.when(step == NZ)
                 def _():
                     def send(j, _):
-                        place = part * HALF + j
+                        place = part * HALF + lax.rem(position_here + j, HALF)
                         peer = at_position(place)
 
                         @pl.when(peer != ep)

time: 147 us -> 146 us (level)
  no operation moved by 1% of the time
where the time goes in v5:
time: 146 us; the launch traced here: 145 us
  Pallas kernels  144 us (99%)
    pallas_call x1, Pallas kernels, body(): pl.pallas_call(kernel, out_shape=(jax.ShapeDtypeStruct((2, rows // (2 * N...  142 us

profile of v5, /device:TPU:6, one launch (start us, length us, event | category | flops | bytes accessed | tf_op | source)
XLA Modules:
  0.0 144.9 jit_solution(15993920657602941038)
XLA Ops:
  0.6 141.8 %shard_map.149 = (bf16[2,8,1024]{2,1,0:T(8,128)(2,1)}, bf16[2,128,256]{2,1,0:T(8,128)(2,1)}, bf16[16,16,2048]{2,1,0:T(8,128)(2,1)}) custom-call(bf16[128,128]{1,0:T(8,128)(2,1)} %query_hbm.1, bf16[128,128]{1,0:T(8,128)(2,1)} %key_hbm.1, bf16[128,128]{1,0:T(8,128)(2,1)} %value_hbm.1, f32[1,64]{1,0:T(1,128)} %bitcast.20, f32[1,64]{1,0:T(1,128)} %bitcast.21, ...), custom_call_target="tpu_custom_call" | custom-call | tf_op jit(solution)/shard_map/pallas_call | solution.py:595
  142.5 2.4 %shard_map.150 = (bf16[128,2048]{1,0:T(8,128)(2,1)}, bf16[8,2048]{1,0:T(8,128)(2,1)}) custom-call(bf16[2,128,256]{2,1,0:T(8,128)(2,1)} %get-tuple-element.7.blend_ref, bf16[256,2048]{1,0:T(8,128)(2,1)} %bitcast.13, bf16[2,8,1024]{2,1,0:T(8,128)(2,1)} %get-tuple-element.9.attn_ref), custom_call_target="tpu_custom_call" | custom-call | tf_op jit(solution)/shard_map/pallas_call | solution.py:673
